TPU v7x, 32 devices: a whole 2x2x4 slice. The times are simulated.
32 devices in a mesh: ep: 8 (over z, x), tp: 4 (over y, core).
Axes of the slice: x: 2, y: 2, z: 4, core: 2. Of those that a mesh axis runs over, the one named last changes fastest.
Arguments:
- blender_incoming_features: bfloat16 [2048, 4096], P('ep', 'tp'), may hold values from -6 to 6
- entry_latent_matrix: bfloat16 [2048, 2048], P('ep', 'tp'), may hold values from -6 to 6
- exit_latent_matrix: bfloat16 [2048, 2048], P('ep', 'tp'), may hold values from -6 to 6
- unactivated_valve: bfloat16 [2048, 4096], P('ep', 'tp'), may hold values from -6 to 6
- presoftplus_strides: float32 [2048, 64], P('ep', 'tp'), may hold values from -7 to 7
- extra_attenuation: float32 [2048, 64], P('ep', 'tp'), may hold values from -1 to 0
- incoming_feature_kernel: bfloat16 [4, 4096], P(None, 'tp'), may hold values from -3 to 3
- entry_latent_kernel: bfloat16 [4, 2048], P(None, 'tp'), may hold values from -3 to 3
- exit_latent_kernel: bfloat16 [4, 2048], P(None, 'tp'), may hold values from -3 to 3
- stride_offset_vector: float32 [64], P('tp'), may hold values from -1 to 1
- attenuation_speed_exponent: float32 [64], P('tp'), may hold values from -16 to -3
- bypass_coef_vector: float32 [64], P('tp'), may hold values from 0.5 to 4
- cluster_rescale_coefs: bfloat16 [4096], P('tp'), may hold values from 0.099609375 to 1.8984375
- blender_result_matrix: bfloat16 [4096, 2048], P('tp'), may hold values from -0.09375 to 0.09375
- latter_microbatch_activations: bfloat16 [2048, 2048], P('ep'), may hold values from -6 to 6
- specialist_rescale_coefs: bfloat16 [2048], replicated, may hold values from 0.099609375 to 1.8984375
- specialist_valve_matrix: bfloat16 [8, 2048, 4096], P('ep', None, 'tp'), may hold values from -0.125 to 0.125
- specialist_expand_matrix: bfloat16 [8, 2048, 4096], P('ep', None, 'tp'), may hold values from -0.125 to 0.125
- specialist_contract_matrix: bfloat16 [8, 4096, 2048], P('ep', 'tp'), may hold values from -0.125 to 0.125
- specialist_picks: int32 [2048, 2], P('ep'), may hold values from 0 to 7, all different within a row; in each aligned block of 256 rows (0 to 255, 256 to 511, ...) at most 96 rows name the same one
- selected_specialist_coefs: float32 [2048, 2], P('ep'), may hold values from 0.1 to 1
Outputs:
- mixed_a: bfloat16 [2048, 2048], P(('ep', 'tp'))
- mixed_b: bfloat16 [2048, 2048], P('ep', 'tp')
Inputs may be any that keep to these rules, and one draw needn't show every extreme that they name: `specialist_picks`: in each aligned block of 256 rows, the rows of one index of ep, no expert is named by more than 96 rows, a bound that some block reaches.
All inputs are finite; a program needn't handle non-finite values.
Results may differ from a plain program's by a relative error of at most 0.019.
Values may be sent and summed in bfloat16 or wider, within the bound.
A program may use at most 64 MiB of HBM per device.

v0:
```python
import functools

import jax
import jax.numpy as jnp
from jax import lax
from jax.experimental import pallas as pl
from jax.experimental.pallas import tpu as pltpu
from jax.sharding import PartitionSpec as P

HEADS = 64
HEAD_DIM = 64
SHARING_CLUSTERS = 16
STATE = 128
BLOCK = 64
TOPK = 2


NORM_EPS = 1e-06
HIGHEST = lax.Precision.HIGHEST


def from_behind(block, axis, distance):
    devices = range(lax.axis_size(axis))
    route = [(i - distance, i) for i in devices if i - distance in devices]
    return lax.ppermute(block, axis, route)


VMEM = pl.BlockSpec(memory_space=pltpu.VMEM)
HALO = 8
LANES = 128


def silu(v):
    return v / (1.0 + jnp.exp(-v))


def widen(per_head, first, count, rows):
    lane = lax.broadcasted_iota(jnp.int32, (rows, LANES), 1)
    pieces = []
    for h in range(first, first + count, 2):
        left = jnp.broadcast_to(per_head[:, h : h + 1], (rows, LANES))
        right = jnp.broadcast_to(per_head[:, h + 1 : h + 2], (rows, LANES))
        pieces.append(jnp.where(lane < HEAD_DIM, left, right))
    return jnp.concatenate(pieces, axis=1)


def ssd_kernel(
    members,
    x_ref,
    b_ref,
    c_ref,
    rim_ref,
    pre_ref,
    extra_ref,
    kx_ref,
    kb_ref,
    kc_ref,
    offset_ref,
    speed_ref,
    bypass_ref,
    y_ref,
    cc_ref,
    run_ref,
    pieces_ref,
    joined,
    state,
):
    rows, channels = x_ref.shape
    latent = b_ref.shape[1]
    groups = latent // STATE
    wide = members * HEAD_DIM
    taps = kx_ref.shape[0]
    ep_count, piece = pieces_ref.shape[0], pieces_ref.shape[1] - 2

    def conv(ref, k_ref, start, width, rim_start):
        joined[0:HALO, 0:width] = rim_ref[:, rim_start : rim_start + width].astype(jnp.float32)
        joined[HALO : HALO + rows, 0:width] = ref[:, start : start + width].astype(jnp.float32)
        kernel = k_ref[:, start : start + width].astype(jnp.float32)
        total = None
        for j in range(taps):
            at = HALO - taps + 1 + j
            term = kernel[j : j + 1] * joined[at : at + rows, 0:width]
            total = term if total is None else total + term
        return silu(total)

    z = pre_ref[...] + offset_ref[...]
    step = jnp.maximum(z, 0.0) + jnp.log1p(jnp.exp(-jnp.abs(z)))
    decay = -jnp.exp(speed_ref[...]) * step + extra_ref[...]
    row = lax.broadcasted_iota(jnp.int32, (rows, rows), 0)
    col = lax.broadcasted_iota(jnp.int32, (rows, rows), 1)
    causal = row >= col
    tri = causal.astype(jnp.float32)
    run = jnp.dot(tri, decay, preferred_element_type=jnp.float32, precision=HIGHEST)
    run_t = lax.dot_general(
        decay,
        tri,
        (((0,), (1,)), ((), ())),
        preferred_element_type=jnp.float32,
        precision=HIGHEST,
    )
    run_ref[...] = run
    last = run[rows - 1 : rows]
    to_end = jnp.exp(last - run)
    bypass = bypass_ref[...]
    lane = lax.broadcasted_iota(jnp.int32, (rows, LANES), 1)
    for g in range(groups):
        first = g * members
        cols = slice(g * wide, (g + 1) * wide)
        xc = conv(x_ref, kx_ref, g * wide, wide, g * wide)
        bb = conv(b_ref, kb_ref, g * STATE, STATE, channels + g * STATE).astype(jnp.bfloat16)
        cc = conv(c_ref, kc_ref, g * STATE, STATE, channels + latent + g * STATE).astype(jnp.bfloat16)
        cc_ref[:, g * STATE : (g + 1) * STATE] = cc
        xs = xc * widen(step, first, members, rows)
        xs16 = xs.astype(jnp.bfloat16)
        scores = lax.dot_general(
            cc, bb, (((1,), (1,)), ((), ())), preferred_element_type=jnp.float32
        )
        scores = jnp.where(causal, scores, 0.0)
        inside = []
        for pair in range(0, members, 2):
            x_pair = xs16[:, pair * HEAD_DIM : (pair + 2) * HEAD_DIM]
            both = []
            for h in (first + pair, first + pair + 1):
                gap = jnp.minimum(run[:, h : h + 1] - run_t[h : h + 1, :], 0.0)
                weights = (jnp.exp(gap) * scores).astype(jnp.bfloat16)
                both.append(jnp.dot(weights, x_pair, preferred_element_type=jnp.float32))
            inside.append(jnp.where(lane < HEAD_DIM, both[0], both[1]))
        y_ref[:, cols] = jnp.concatenate(inside, axis=1) + xc * widen(bypass, first, members, 1)
        x_end = (xs * widen(to_end, first, members, rows)).astype(jnp.bfloat16)
        state[:, cols] = lax.dot_general(
            bb, x_end, (((0,), (0,)), ((), ())), preferred_element_type=jnp.float32
        )
    for e in range(ep_count):
        pieces_ref[e, 0:piece, :] = state[e * piece : (e + 1) * piece, :].astype(jnp.bfloat16)
    logs = widen(last, 0, groups * members, 1)
    high = logs.astype(jnp.bfloat16)
    low = (logs - high.astype(jnp.float32)).astype(jnp.bfloat16)
    for e in range(ep_count):
        pieces_ref[e, piece : piece + 1, :] = high
        pieces_ref[e, piece + 1 : piece + 2, :] = low


def prefix_kernel(in_ref, out_ref):
    ep_count, piece = in_ref.shape[0], in_ref.shape[1] - 2
    entering = jnp.zeros((piece, in_ref.shape[2]), jnp.float32)
    for d in range(ep_count):
        out_ref[d, :, :] = entering.astype(jnp.bfloat16)
        block = in_ref[d, :, :].astype(jnp.float32)
        log = block[piece : piece + 1] + block[piece + 1 : piece + 2]
        entering = entering * jnp.exp(log) + block[0:piece]


def finish_kernel(
    members, y_ref, cc_ref, run_ref, enter_ref, valve_ref, gain_ref, w_ref, out_ref, normed
):
    rows, channels = y_ref.shape
    wide = members * HEAD_DIM

    @pl.when(pl.program_id(0) == 0)
    def _():
        grown = jnp.exp(run_ref[...])
        for g in range(channels // wide):
            cols = slice(g * wide, (g + 1) * wide)
            carried = jnp.dot(
                cc_ref[:, g * STATE : (g + 1) * STATE],
                enter_ref[:, cols],
                preferred_element_type=jnp.float32,
            )
            ssd = y_ref[:, cols] + carried * widen(grown, g * members, members, rows)
            gated = ssd * silu(valve_ref[:, cols].astype(jnp.float32))
            scale = lax.rsqrt(jnp.mean(gated * gated, axis=1, keepdims=True) + NORM_EPS)
            normed[:, cols] = (gated * scale * gain_ref[:, cols].astype(jnp.float32)).astype(
                jnp.bfloat16
            )

    out_ref[...] = jnp.dot(
        normed[...], w_ref[...], preferred_element_type=jnp.float32
    ).astype(jnp.bfloat16)


def experts_kernel(x_ref, gate_ref, up_ref, down_ref, out_ref, total):
    step = pl.program_id(1)
    parts, _, depth = x_ref.shape
    gate = up = 0.0
    for p in range(parts):
        rows = x_ref[p]
        deep = slice(p * depth, (p + 1) * depth)
        gate += jnp.dot(rows, gate_ref[deep, :], preferred_element_type=jnp.float32)
        up += jnp.dot(rows, up_ref[deep, :], preferred_element_type=jnp.float32)
    hidden = (silu(gate) * up).astype(jnp.bfloat16)
    term = jnp.dot(hidden, down_ref[...], preferred_element_type=jnp.float32)
    final = pl.num_programs(1) - 1

    @pl.when(step == 0)
    def _():
        total[...] = term

    @pl.when(step > 0)
    def _():
        total[...] += term

    @pl.when(step == final)
    def _():
        for p in range(parts):
            out_ref[p] = total[:, p * depth : (p + 1) * depth].astype(jnp.bfloat16)


def run_experts(rows, gate, up, down):
    parts, experts, count, depth = rows.shape
    width = parts * depth
    units = gate.shape[2]
    tile = min(256, units)
    return pl.pallas_call(
        experts_kernel,
        grid=(experts, units // tile),
        in_specs=[
            pl.BlockSpec((parts, None, count, depth), lambda e, f: (0, e, 0, 0)),
            pl.BlockSpec((None, width, tile), lambda e, f: (e, 0, f)),
            pl.BlockSpec((None, width, tile), lambda e, f: (e, 0, f)),
            pl.BlockSpec((None, tile, width), lambda e, f: (e, f, 0)),
        ],
        out_specs=pl.BlockSpec((parts, None, count, depth), lambda e, f: (0, e, 0, 0)),
        out_shape=jax.ShapeDtypeStruct((parts, experts, count, depth), jnp.bfloat16),
        scratch_shapes=[pltpu.VMEM((count, width), jnp.float32)],
        cost_estimate=pl.CostEstimate(
            flops=6 * experts * count * width * units,
            bytes_accessed=2 * experts * (2 * count * width + 3 * width * units),
            transcendentals=experts * count * units,
        ),
        compiler_params=pltpu.CompilerParams(
            dimension_semantics=("arbitrary", "arbitrary"), vmem_limit_bytes=48 * 1024 * 1024
        ),
        name="experts",
    )(rows, gate, up, down)


def local(
    blender_incoming_features,
    entry_latent_matrix,
    exit_latent_matrix,
    unactivated_valve,
    presoftplus_strides,
    extra_attenuation,
    incoming_feature_kernel,
    entry_latent_kernel,
    exit_latent_kernel,
    stride_offset_vector,
    attenuation_speed_exponent,
    bypass_coef_vector,
    cluster_rescale_coefs,
    blender_result_matrix,
    latter_microbatch_activations,
    specialist_rescale_coefs,
    specialist_valve_matrix,
    specialist_expand_matrix,
    specialist_contract_matrix,
    specialist_picks,
    selected_specialist_coefs,
):
    tap_count = incoming_feature_kernel.shape[0]
    tok_rows = blender_incoming_features.shape[0]
    members_within_cluster = HEADS // SHARING_CLUSTERS
    ep_count = lax.axis_size("ep")
    channels = blender_incoming_features.shape[1]
    latent = entry_latent_matrix.shape[1]
    heads_local = presoftplus_strides.shape[1]
    piece = STATE // ep_count
    tail = tok_rows - HALO
    rim = from_behind(
        jnp.concatenate(
            [
                blender_incoming_features[tail:],
                entry_latent_matrix[tail:],
                exit_latent_matrix[tail:],
            ],
            axis=1,
        ),
        "ep",
        1,
    )
    block_out, conv_c_out, running, pieces = pl.pallas_call(
        functools.partial(ssd_kernel, members_within_cluster),
        in_specs=[VMEM] * 12,
        out_specs=[VMEM] * 4,
        out_shape=[
            jax.ShapeDtypeStruct((tok_rows, channels), jnp.float32),
            jax.ShapeDtypeStruct((tok_rows, latent), jnp.bfloat16),
            jax.ShapeDtypeStruct((tok_rows, heads_local), jnp.float32),
            jax.ShapeDtypeStruct((ep_count, piece + 2, channels), jnp.bfloat16),
        ],
        scratch_shapes=[
            pltpu.VMEM((tok_rows + HALO, members_within_cluster * HEAD_DIM), jnp.float32),
            pltpu.VMEM((STATE, channels), jnp.float32),
        ],
        cost_estimate=pl.CostEstimate(
            flops=2 * tok_rows * tok_rows * channels * 64,
            bytes_accessed=6 * tok_rows * channels * 2,
            transcendentals=tok_rows * tok_rows * heads_local,
        ),
        name="ssd_local",
    )(
        blender_incoming_features,
        entry_latent_matrix,
        exit_latent_matrix,
        rim,
        presoftplus_strides,
        extra_attenuation,
        incoming_feature_kernel,
        entry_latent_kernel,
        exit_latent_kernel,
        stride_offset_vector[None, :],
        attenuation_speed_exponent[None, :],
        bypass_coef_vector[None, :],
    )
    token_count = latter_microbatch_activations.shape[0]
    model_width = latter_microbatch_activations.shape[1]
    local_experts = specialist_valve_matrix.shape[0]
    expert_count = ep_count * local_experts
    capacity = 3 * token_count * TOPK // (2 * expert_count)
    slot_total = expert_count * capacity
    widened = latter_microbatch_activations.astype(jnp.float32)
    share = model_width // lax.axis_size("tp")
    own = lax.axis_index("tp") * share
    normed_b = (
        lax.dynamic_slice_in_dim(latter_microbatch_activations, own, share, 1).astype(jnp.float32)
        * lax.rsqrt(jnp.mean(widened * widened, axis=-1, keepdims=True) + NORM_EPS)
        * lax.dynamic_slice_in_dim(specialist_rescale_coefs, own, share, 0).astype(jnp.float32)
    ).astype(jnp.bfloat16)
    flat_routes = specialist_picks.reshape(-1)
    assigned = flat_routes.shape[0]
    positions = jnp.arange(assigned, dtype=jnp.int32)
    earlier_same = (flat_routes[:, None] == flat_routes[None, :]) & (
        positions[None, :] < positions[:, None]
    )
    slot_rank = jnp.sum(earlier_same.astype(jnp.int32), axis=1)
    slot_of = flat_routes * capacity + slot_rank
    slot_ids = jnp.arange(slot_total, dtype=jnp.int32)
    placing = (slot_ids[:, None] == slot_of[None, :]).astype(jnp.bfloat16)
    placing = jnp.sum(placing.reshape(slot_total, token_count, TOPK), axis=2)
    outgoing = jnp.dot(placing, normed_b, preferred_element_type=jnp.float32).astype(jnp.bfloat16)
    outgoing = outgoing.reshape(ep_count, local_experts, capacity, share)
    chunks = 2 if capacity % 32 == 0 else 1
    size = capacity // chunks
    gathered = []
    for k in range(chunks):
        arrived = lax.all_to_all(
            outgoing[:, :, k * size : (k + 1) * size],
            "ep",
            split_axis=0,
            concat_axis=0,
            tiled=True,
        )
        arrived_rows = arrived.transpose(1, 0, 2, 3).reshape(local_experts, ep_count * size, share)
        gathered.append(lax.all_gather(arrived_rows, "tp"))
    spread = None
    partials = []
    for k in range(chunks):
        if spread is None:
            gathered[k], pieces = lax.optimization_barrier((gathered[k], pieces))
        else:
            gathered[k], spread = lax.optimization_barrier((gathered[k], spread))
        partial_out = run_experts(
            gathered[k],
            specialist_valve_matrix,
            specialist_expand_matrix,
            specialist_contract_matrix,
        )
        if spread is None:
            partial_out, pieces = lax.optimization_barrier((partial_out, pieces))
            spread = lax.all_to_all(pieces, "ep", split_axis=0, concat_axis=0, tiled=True)
        else:
            partial_out, spread = lax.optimization_barrier((partial_out, spread))
        partials.append(partial_out)
    back = []
    for k in range(chunks):
        summed = lax.psum_scatter(partials[k], "tp", scatter_dimension=0, tiled=False)
        summed = summed.reshape(local_experts, ep_count, size, share).transpose(1, 0, 2, 3)
        back.append(lax.all_to_all(summed, "ep", split_axis=0, concat_axis=0, tiled=True))
    returned = back[0] if chunks == 1 else jnp.concatenate(back, axis=2)
    entering = pl.pallas_call(
        prefix_kernel,
        in_specs=[VMEM],
        out_specs=VMEM,
        out_shape=jax.ShapeDtypeStruct((ep_count, piece, channels), jnp.bfloat16),
        name="state_prefix",
    )(spread)
    enter_state = lax.all_to_all(entering, "ep", split_axis=0, concat_axis=0, tiled=True).reshape(
        STATE, channels
    )
    width_a = blender_result_matrix.shape[1]
    tile_a = min(512, width_a)
    whole = lambda *shape: pl.BlockSpec(shape, lambda i: (0,) * len(shape))
    partial_a = pl.pallas_call(
        functools.partial(finish_kernel, members_within_cluster),
        grid=(width_a // tile_a,),
        in_specs=[
            whole(tok_rows, channels),
            whole(tok_rows, latent),
            whole(tok_rows, heads_local),
            whole(STATE, channels),
            whole(tok_rows, channels),
            whole(1, channels),
            pl.BlockSpec((channels, tile_a), lambda i: (0, i)),
        ],
        out_specs=pl.BlockSpec((tok_rows, tile_a), lambda i: (0, i)),
        out_shape=jax.ShapeDtypeStruct((tok_rows, width_a), jnp.bfloat16),
        scratch_shapes=[pltpu.VMEM((tok_rows, channels), jnp.bfloat16)],
        cost_estimate=pl.CostEstimate(
            flops=8 * tok_rows * channels * (width_a + 4 * STATE),
            bytes_accessed=2 * channels * (width_a + 4 * tok_rows) + 2 * tok_rows * width_a,
            transcendentals=2 * tok_rows * channels,
        ),
        compiler_params=pltpu.CompilerParams(dimension_semantics=("arbitrary",)),
        name="finish_mixer",
    )(
        block_out,
        conv_c_out,
        running,
        enter_state,
        unactivated_valve,
        cluster_rescale_coefs[None, :],
        blender_result_matrix,
    )
    mixed_a = lax.psum_scatter(partial_a, "tp", scatter_dimension=0, tiled=True)
    returned = returned.reshape(slot_total, -1)
    token_slots = slot_of.reshape(token_count, TOPK)
    combined = jnp.zeros((token_count, returned.shape[1]), jnp.float32)
    for pick_index in range(TOPK):
        selecting = (token_slots[:, pick_index][:, None] == slot_ids[None, :]).astype(jnp.bfloat16)
        chosen_rows = jnp.dot(selecting, returned, preferred_element_type=jnp.float32)
        combined = combined + chosen_rows * selected_specialist_coefs[:, pick_index][:, None]
    mixed_b = combined.astype(jnp.bfloat16)
    return (mixed_a, mixed_b)


def solution(mesh):
    in_specs = (
        P("ep", "tp"),
        P("ep", "tp"),
        P("ep", "tp"),
        P("ep", "tp"),
        P("ep", "tp"),
        P("ep", "tp"),
        P(None, "tp"),
        P(None, "tp"),
        P(None, "tp"),
        P("tp"),
        P("tp"),
        P("tp"),
        P("tp"),
        P("tp", None),
        P("ep", None),
        P(),
        P("ep", None, "tp"),
        P("ep", None, "tp"),
        P("ep", "tp", None),
        P("ep", None),
        P("ep", None),
    )
    out_specs = (P(("ep", "tp"), None), P("ep", "tp"))
    return jax.shard_map(local, mesh=mesh, in_specs=in_specs, out_specs=out_specs, check_vma=False)
```

profile of v0, /device:TPU:0, one launch (start us, length us, event | category | flops | bytes accessed | tf_op | source)
XLA Modules:
  0.0 168.0 jit_solution(4160533942991711649)
XLA Ops:
  7.2 0.0 all-gather.5.cloned.1.call-start
  7.2 0.8 copy.57
  8.0 0.1 eq.60
  8.2 0.3 convert_reduce_fusion
  8.4 0.1 reduce_sum.33
  8.6 0.1 copy.58
  8.7 0.7 multiply_add_fusion
  9.4 0.3 fusion.4
  9.7 1.5 multiply_reduce_fusion
  11.2 0.8 dynamic-slice_convert_fusion
  12.0 1.4 convolution_convert_fusion
  13.4 0.1 fusion.11
  13.5 0.0 slice-start
  13.5 0.0 slice-start.1
  13.5 0.0 slice-start.2
  13.5 0.0 copy-start.4
  13.5 0.0 copy-start.5
  13.5 19.4 %all_to_all.30 = bf16[8,1,48,512]{3,2,1,0:T(8,128)(2,1)} all-to-all(bf16[8,1,48,512]{3,2,1,0:T(8,128)(2,1)S(1)} %get-tuple-element.26), channel_id=1, replica_groups=mesh['ep'=8,'tp'=4] {'ep'}, dimensions={0} | all-to-all | bytes 786432 | tf_op jit(solution)/shard_map/all_to_all | solution.py:346
  32.9 0.0 all-gather.5.cloned.1.call-update
  32.9 0.0 all-gather.3.cloned.1.call-start
  33.0 15.1 %all_to_all.31 = bf16[8,1,48,512]{3,2,1,0:T(8,128)(2,1)} all-to-all(bf16[8,1,48,512]{3,2,1,0:T(8,128)(2,1)S(1)} %get-tuple-element.27), channel_id=1, replica_groups=mesh['ep'=8,'tp'=4] {'ep'}, dimensions={0} | all-to-all | bytes 786432 | tf_op jit(solution)/shard_map/all_to_all | solution.py:346
  48.1 0.0 all-gather.3.cloned.1.call-update
  48.1 0.0 reduce-scatter.6.cloned.1.call-start
  48.1 0.0 slice-done
  48.1 0.0 slice-done.1
  48.1 0.0 slice-done.2
  48.2 3.0 %collective-permute-start = (bf16[8,2048]{1,0:T(8,128)(2,1)S(1)}, bf16[8,2048]{1,0:T(8,128)(2,1)S(1)}, u32[]{:S(2)}, u32[]{:S(2)}) collective-permute-start(bf16[8,2048]{1,0:T(8,128)(2,1)S(1)} %pad_maximum_fusion.1), channel_id=1, source_target_pairs={{0,4},{4,8},{8,12},{12,16},{16,20},{20,24},{24,28},{1,5},{5,9},{9,... | collective-permute-start | bytes 98312 | tf_op jit(solution)/shard_map/ppermute | solution.py:25
  51.2 0.0 copy-done.4
  51.2 0.8 copy.55.pre_ref
  51.9 0.0 copy-done.5
  51.9 0.8 copy.56.extra_ref
  52.7 0.1 collective-permute-done.rim_ref
  52.8 0.6 copy-done.8
  53.4 6.4 %ssd_local.1 = (f32[256,1024]{1,0:T(8,128)}, bf16[256,512]{1,0:T(8,128)(2,1)}, f32[256,16]{1,0:T(8,128)}, bf16[8,18,1024]{2,1,0:T(8,128)(2,1)}) custom-call(bf16[256,1024]{1,0:T(8,128)(2,1)} %x_ref.1, bf16[256,512]{1,0:T(8,128)(2,1)} %b_ref.1, bf16[256,512]{1,0:T(8,128)(2,1)} %c_ref.1, bf16[8,2048]{1,0:T(8,128)(2,1)} %copy-done.8, f32[256,16]{1,0:T(8,128)} %copy.55.pre_ref, ...), custom_call_target="tpu_custom_call" | custom-call | flops 8589934592 | bytes 3145728 | tf_op jit(solution)/shard_map/ssd_local/pallas_call | solution.py:281
  59.8 1.6 copy-done.1
  61.5 10.3 %experts.2 = bf16[4,1,384,512]{3,2,1,0:T(8,128)(2,1)} custom-call(bf16[4,1,384,512]{3,2,1,0:T(8,128)(2,1)S(1)} %copy-done.1, bf16[1,2048,1024]{2,1,0:T(8,128)(2,1)} %gate_ref.3, bf16[1,2048,1024]{2,1,0:T(8,128)(2,1)} %up_ref.3, bf16[1,1024,2048]{2,1,0:T(8,128)(2,1)} %down_ref.3), custom_call_target="tpu_custom_call" | custom-call | flops 4831838208 | bytes 15728640 | tf_op jit(solution)/shard_map/experts/pallas_call | solution.py:213
  71.8 0.0 reduce-scatter.6.cloned.1.call-update
  71.8 4.7 %all-to-all-start.2 = ((bf16[8,18,1024]{2,1,0:T(8,128)(2,1)}), bf16[8,18,1024]{2,1,0:T(8,128)(2,1)S(1)}, u32[]{:S(2)}, u32[]{:S(2)}) async-start(bf16[8,18,1024]{2,1,0:T(8,128)(2,1)} %get-tuple-element.20), calls=%async_computation.2 | async-start | bytes 786432 | tf_op jit(solution)/shard_map/all_to_all | solution.py:370
  76.5 0.0 reduce-scatter.8.cloned.1.call-start
  76.6 0.0 all-gather.3.cloned.1.call-done.x_ref
  76.6 10.0 %all-to-all-done.2.in_ref = bf16[8,18,1024]{2,1,0:T(8,128)(2,1)S(1)} async-done(((bf16[8,18,1024]{2,1,0:T(8,128)(2,1)}), bf16[8,18,1024]{2,1,0:T(8,128)(2,1)S(1)}, u32[]{:S(2)}, u32[]{:S(2)}) %all-to-all-start.2) | async-done | bytes 294944 | tf_op jit(solution)/shard_map/all_to_all | solution.py:370
  86.6 1.4 copy-done
  88.0 10.5 %experts.3 = bf16[4,1,384,512]{3,2,1,0:T(8,128)(2,1)} custom-call(bf16[4,1,384,512]{3,2,1,0:T(8,128)(2,1)S(1)} %copy-done, bf16[1,2048,1024]{2,1,0:T(8,128)(2,1)} %gate_ref.3, bf16[1,2048,1024]{2,1,0:T(8,128)(2,1)} %up_ref.3, bf16[1,1024,2048]{2,1,0:T(8,128)(2,1)} %down_ref.3), custom_call_target="tpu_custom_call" | custom-call | flops 4831838208 | bytes 15728640 | tf_op jit(solution)/shard_map/experts/pallas_call | solution.py:213
  98.4 0.0 copy-done.2
  98.4 0.0 reduce-scatter.8.cloned.1.call-update
  98.5 1.8 %state_prefix.1 = bf16[8,16,1024]{2,1,0:T(8,128)(2,1)} custom-call(bf16[8,18,1024]{2,1,0:T(8,128)(2,1)} %copy-done.2), custom_call_target="tpu_custom_call" | custom-call | tf_op jit(solution)/shard_map/state_prefix/pallas_call | solution.py:380
  100.3 3.8 %all-to-all-start.3 = ((bf16[8,16,1024]{2,1,0:T(8,128)(2,1)}), bf16[8,16,1024]{2,1,0:T(8,128)(2,1)S(1)}, u32[]{:S(2)}, u32[]{:S(2)}) async-start(bf16[8,16,1024]{2,1,0:T(8,128)(2,1)} %state_prefix.1), calls=%async_computation.3 | async-start | bytes 524288 | tf_op jit(solution)/shard_map/all_to_all | solution.py:387
  104.0 0.0 reduce-scatter.4.cloned.1.call-start
  104.1 0.0 copy-done.6
  104.1 0.6 broadcast_in_dim.11.gain_ref
  104.7 7.8 %all-to-all-done.3 = bf16[8,16,1024]{2,1,0:T(8,128)(2,1)S(1)} async-done(((bf16[8,16,1024]{2,1,0:T(8,128)(2,1)}), bf16[8,16,1024]{2,1,0:T(8,128)(2,1)S(1)}, u32[]{:S(2)}, u32[]{:S(2)}) %all-to-all-start.3) | async-done | bytes 262176 | tf_op jit(solution)/shard_map/all_to_all | solution.py:387
  112.5 0.7 copy-done.3
  113.2 6.7 %finish_mixer.1 = bf16[256,2048]{1,0:T(8,128)(2,1)} custom-call(f32[256,1024]{1,0:T(8,128)} %get-tuple-element.14.y_ref, bf16[256,512]{1,0:T(8,128)(2,1)} %get-tuple-element.15.cc_ref, f32[256,16]{1,0:T(8,128)} %get-tuple-element.16.run_ref, bf16[128,1024]{1,0:T(8,128)(2,1)} %bitcast.31, bf16[256,1024]{1,0:T(8,128)(2,1)} %valve_ref.1, ...), custom_call_target="tpu_custom_call" | custom-call | flops 5368709120 | bytes 7340032 | tf_op jit(solution)/shard_map/finish_mixer/pallas_call | solution.py:393
  119.8 0.0 reduce-scatter.4.cloned.1.call-update
  119.9 0.0 reduce-scatter.6.cloned.1.call-done
  119.9 3.5 %all-to-all-start.4 = ((bf16[8,1,48,512]{3,2,1,0:T(8,128)(2,1)}), bf16[8,1,48,512]{3,2,1,0:T(8,128)(2,1)S(1)}, u32[]{:S(2)}, u32[]{:S(2)}) async-start(bf16[8,1,48,512]{3,2,1,0:T(8,128)(2,1)} %bitcast.29), calls=%async_computation.6 | async-start | bytes 786432 | tf_op jit(solution)/shard_map/all_to_all | solution.py:378
  123.4 10.3 %reduce-scatter.8.cloned.1.call-done = bf16[1,1,384,512]{3,2,1,0:T(8,128)(2,1)} async-done(((bf16[4,1,384,512]{3,2,1,0:T(8,128)(2,1)}), bf16[1,1,384,512]{3,2,1,0:T(8,128)(2,1)}) %reduce-scatter.8.cloned.1.call-update) | async-done | bytes 393232 | tf_op jit(solution)/shard_map/reduce_scatter | solution.py:376
  133.7 1.1 all-to-all-done.4
  134.8 4.4 %all-to-all-start.5 = ((bf16[8,1,48,512]{3,2,1,0:T(8,128)(2,1)}), bf16[8,1,48,512]{3,2,1,0:T(8,128)(2,1)S(1)}, u32[]{:S(2)}, u32[]{:S(2)}) async-start(bf16[8,1,48,512]{3,2,1,0:T(8,128)(2,1)} %bitcast.30), calls=%async_computation.8 | async-start | bytes 786432 | tf_op jit(solution)/shard_map/all_to_all | solution.py:378
  139.2 11.5 %all-to-all-done.5 = bf16[8,1,48,512]{3,2,1,0:T(8,128)(2,1)S(1)} async-done(((bf16[8,1,48,512]{3,2,1,0:T(8,128)(2,1)}), bf16[8,1,48,512]{3,2,1,0:T(8,128)(2,1)S(1)}, u32[]{:S(2)}, u32[]{:S(2)}) %all-to-all-start.5) | async-done | bytes 393248 | tf_op jit(solution)/shard_map/all_to_all | solution.py:378
  150.7 0.1 pad_maximum_fusion
  150.8 0.4 convolution_multiply_fusion.1
  151.2 1.1 fusion.2
  152.4 9.1 %reduce-scatter.4.cloned.1.call-done = bf16[64,2048]{1,0:T(8,128)(2,1)} async-done(((bf16[256,2048]{1,0:T(8,128)(2,1)}), bf16[64,2048]{1,0:T(8,128)(2,1)}) %reduce-scatter.4.cloned.1.call-update) | async-done | bytes 262160 | tf_op jit(solution)/shard_map/reduce_scatter | solution.py:424
  (13 shorter events, 0.0 us)
Async XLA Ops:
  7.2 52.7 %all-gather.5.cloned.1.call-start = ((), (), s32[]{:S(2)}) async-start(), calls=%async_computation.10 | async-start | bytes 1966080 | tf_op jit(solution)/shard_map/all_gather | solution.py:354
  13.5 34.7 %slice-start = ((bf16[256,1024]{1,0:T(8,128)(2,1)}), bf16[8,1024]{1,0:T(8,128)(2,1)S(1)}, s32[]{:S(2)}) async-start(bf16[256,1024]{1,0:T(8,128)(2,1)} %x_ref.1), calls=%async_computation.14 | async-start | bytes 32768 | tf_op jit(solution)/shard_map/slice | solution.py:272
  13.5 34.7 %slice-start.1 = ((bf16[256,512]{1,0:T(8,128)(2,1)}), bf16[8,512]{1,0:T(8,128)(2,1)S(1)}, s32[]{:S(2)}) async-start(bf16[256,512]{1,0:T(8,128)(2,1)} %c_ref.1), calls=%async_computation.15 | async-start | bytes 16384 | tf_op jit(solution)/shard_map/slice | solution.py:274
  13.5 34.7 %slice-start.2 = ((bf16[256,512]{1,0:T(8,128)(2,1)}), bf16[8,512]{1,0:T(8,128)(2,1)S(1)}, s32[]{:S(2)}) async-start(bf16[256,512]{1,0:T(8,128)(2,1)} %b_ref.1), calls=%async_computation.16 | async-start | bytes 16384 | tf_op jit(solution)/shard_map/slice | solution.py:273
  13.5 37.7 %copy-start.4 = (f32[256,16]{0,1:T(8,128)S(1)}, f32[256,16]{0,1:T(8,128)}, u32[]{:S(2)}) copy-start(f32[256,16]{0,1:T(8,128)} %param.25) | copy-start | bytes 49156
  13.5 38.4 %copy-start.5 = (f32[256,16]{0,1:T(8,128)S(1)}, f32[256,16]{0,1:T(8,128)}, u32[]{:S(2)}) copy-start(f32[256,16]{0,1:T(8,128)} %param.26) | copy-start | bytes 49156
  32.9 43.7 %all-gather.3.cloned.1.call-start = ((), (), s32[]{:S(2)}) async-start(), calls=%async_computation.9 | async-start | bytes 1966080 | tf_op jit(solution)/shard_map/all_gather | solution.py:354
  48.1 71.8 %reduce-scatter.6.cloned.1.call-start = ((), (), s32[]{:S(2)}) async-start(), calls=%async_computation.12 | async-start | bytes 1966080 | tf_op jit(solution)/shard_map/reduce_scatter | solution.py:376
  48.2 4.6 %collective-permute-start = (bf16[8,2048]{1,0:T(8,128)(2,1)S(1)}, bf16[8,2048]{1,0:T(8,128)(2,1)S(1)}, u32[]{:S(2)}, u32[]{:S(2)}) collective-permute-start(bf16[8,2048]{1,0:T(8,128)(2,1)S(1)} %pad_maximum_fusion.1), channel_id=1, source_target_pairs={{0,4},{4,8},{8,12},{12,16},{16,20},{20,24},{24,28},{1,5},{5,9},{9,... | collective-permute-start | bytes 98312 | tf_op jit(solution)/shard_map/ppermute | solution.py:25
  52.8 0.6 copy-start.8
  59.8 1.6 copy-start.1
  71.8 14.8 %all-to-all-start.2 = ((bf16[8,18,1024]{2,1,0:T(8,128)(2,1)}), bf16[8,18,1024]{2,1,0:T(8,128)(2,1)S(1)}, u32[]{:S(2)}, u32[]{:S(2)}) async-start(bf16[8,18,1024]{2,1,0:T(8,128)(2,1)} %get-tuple-element.20), calls=%async_computation.2 | async-start | bytes 786432 | tf_op jit(solution)/shard_map/all_to_all | solution.py:370
  76.5 57.1 %reduce-scatter.8.cloned.1.call-start = ((), (), s32[]{:S(2)}) async-start(), calls=%async_computation.13 | async-start | bytes 1966080 | tf_op jit(solution)/shard_map/reduce_scatter | solution.py:376
  86.6 1.4 copy-start
  88.0 10.5 %copy-start.2 = (bf16[8,18,1024]{2,1,0:T(8,128)(2,1)}, bf16[8,18,1024]{2,1,0:T(8,128)(2,1)S(1)}, u32[]{:S(2)}) copy-start(bf16[8,18,1024]{2,1,0:T(8,128)(2,1)S(1)} %all-to-all-done.2.in_ref) | copy-start | bytes 884740
  98.4 5.6 %copy-start.6 = (bf16[1024]{0:T(1024)(128)(2,1)S(1)}, bf16[1024]{0:T(1024)(128)(2,1)}, u32[]{:S(2)}) copy-start(bf16[1024]{0:T(1024)(128)(2,1)} %param.33) | copy-start | bytes 6148
  100.3 12.2 %all-to-all-start.3 = ((bf16[8,16,1024]{2,1,0:T(8,128)(2,1)}), bf16[8,16,1024]{2,1,0:T(8,128)(2,1)S(1)}, u32[]{:S(2)}, u32[]{:S(2)}) async-start(bf16[8,16,1024]{2,1,0:T(8,128)(2,1)} %state_prefix.1), calls=%async_computation.3 | async-start | bytes 524288 | tf_op jit(solution)/shard_map/all_to_all | solution.py:387
  104.0 57.4 %reduce-scatter.4.cloned.1.call-start = ((), (), s32[]{:S(2)}) async-start(), calls=%async_computation.11 | async-start | bytes 1310720 | tf_op jit(solution)/shard_map/reduce_scatter | solution.py:424
  112.5 0.7 copy-start.3
  119.8 19.3 %copy-start.7 = (f32[256,2]{0,1:T(2,128)S(1)}, f32[256,2]{0,1:T(2,128)}, u32[]{:S(2)}) copy-start(f32[256,2]{0,1:T(2,128)} %param.41) | copy-start | bytes 6148
  119.9 14.9 %all-to-all-start.4 = ((bf16[8,1,48,512]{3,2,1,0:T(8,128)(2,1)}), bf16[8,1,48,512]{3,2,1,0:T(8,128)(2,1)S(1)}, u32[]{:S(2)}, u32[]{:S(2)}) async-start(bf16[8,1,48,512]{3,2,1,0:T(8,128)(2,1)} %bitcast.29), calls=%async_computation.6 | async-start | bytes 786432 | tf_op jit(solution)/shard_map/all_to_all | solution.py:378
  134.8 15.9 %all-to-all-start.5 = ((bf16[8,1,48,512]{3,2,1,0:T(8,128)(2,1)}), bf16[8,1,48,512]{3,2,1,0:T(8,128)(2,1)S(1)}, u32[]{:S(2)}, u32[]{:S(2)}) async-start(bf16[8,1,48,512]{3,2,1,0:T(8,128)(2,1)} %bitcast.30), calls=%async_computation.8 | async-start | bytes 786432 | tf_op jit(solution)/shard_map/all_to_all | solution.py:378
Sparse Core Ops, SparseCore 0:
  33.0 18.3 all-gather.4
  53.0 19.6 all-gather.2
  75.2 27.9 reduce-scatter.5
  105.6 28.0 reduce-scatter.7
  136.6 24.7 reduce-scatter.3
where the time goes:
time: 169 us; the launch traced here: 168 us
  waiting for transfers between devices  50 us (30%)
  Pallas kernels  35.7 us (21%)
  blocking collectives  34.5 us (20%)
  starting transfers between devices  19.5 us (12%)
  between operations  14 us (8%)
  local copies, waits for them, and re-layouts  7.76 us (5%)
  other arithmetic  3.63 us (2%)
  matrix products  2.95 us (2%)
    all_to_all x2, blocking collectives, local(): lax.all_to_all(outgoing[:, :, k * size:(k + 1) * size], 'ep', split_axis=...  34.5 us
    pallas_call x2, Pallas kernels, run_experts(): pl.pallas_call(experts_kernel, grid=(experts, units // tile), in_specs=[p...  20.8 us
    all_to_all x2, waiting for transfers between devices, local(): lax.all_to_all(summed, 'ep', split_axis=0, concat_axis=0, tiled=True)  12.7 us
    reduce_scatter x2, waiting for transfers between devices, local(): lax.psum_scatter(partials[k], 'tp', scatter_dimension=0, tiled=False)  10.3 us
    all_to_all x1, waiting for transfers between devices, local(): lax.all_to_all(pieces, 'ep', split_axis=0, concat_axis=0, tiled=True)  9.97 us
    reduce_scatter x1, waiting for transfers between devices, local(): mixed_a = lax.psum_scatter(partial_a, 'tp', scatter_dimension=0, tiled=True)  9.06 us
    all_to_all x2, starting transfers between devices, local(): lax.all_to_all(summed, 'ep', split_axis=0, concat_axis=0, tiled=True)  7.84 us
    all_to_all x1, waiting for transfers between devices, local(): lax.all_to_all(entering, 'ep', split_axis=0, concat_axis=0, tiled=True)  7.81 us
  transfers between devices with their start and end apart: 10, of which 7 were waited for; matrix products, arithmetic and copies ran while one was open for 2% of the time, Pallas kernels for 21%

commit v1 on v0

v1 whole, which is shorter than its diff:
```python
import functools

import jax
import jax.numpy as jnp
from jax import lax
from jax.experimental import pallas as pl
from jax.experimental.pallas import tpu as pltpu
from jax.sharding import PartitionSpec as P

HEADS = 64
HEAD_DIM = 64
SHARING_CLUSTERS = 16
STATE = 128
TOPK = 2

NORM_EPS = 1e-06
HIGHEST = lax.Precision.HIGHEST
MESH = pl.DeviceIdType.MESH
F32 = jnp.float32
BF16 = jnp.bfloat16
HALO = 16
LANES = 128
CHUNKS = 4


def silu(v):
    return v / (1.0 + jnp.exp(-v))


def dot(a, b):
    return jnp.dot(a, b, preferred_element_type=F32)


def dot_last(a, b, precision=None):
    return lax.dot_general(
        a, b, (((1,), (1,)), ((), ())), preferred_element_type=F32, precision=precision
    )


def widen(per_head, first, count, rows):
    lane = lax.broadcasted_iota(jnp.int32, (rows, LANES), 1)
    pieces = []
    for h in range(first, first + count, 2):
        left = jnp.broadcast_to(per_head[:, h : h + 1], (rows, LANES))
        right = jnp.broadcast_to(per_head[:, h + 1 : h + 2], (rows, LANES))
        pieces.append(jnp.where(lane < HEAD_DIM, left, right))
    return jnp.concatenate(pieces, axis=1)


def layer_kernel(
    E,
    T,
    picks_h,
    coefs_h,
    act_h,
    bgain_h,
    x_h,
    b_h,
    c_h,
    kx_h,
    kb_h,
    kc_h,
    pre_h,
    extra_h,
    valve_h,
    again_h,
    wg_h,
    wu_h,
    wd_h,
    wr_h,
    offset_s,
    speed_s,
    bypass_s,
    outa_ref,
    outb_ref,
    picks_v,
    coefs_v,
    act_v,
    bgain_v,
    x_v,
    b_v,
    c_v,
    kx_v,
    kb_v,
    kc_v,
    pre_v,
    extra_v,
    valve_v,
    again_v,
    wg_v,
    wu_v,
    wd_v,
    wr_v,
    nb,
    out,
    X,
    hid,
    tc,
    fc,
    own,
    ys,
    yr,
    fin,
    ret,
    acc,
    cols_v,
    rim,
    joined,
    ybuf,
    cc_v,
    grown_v,
    state,
    st16,
    peerst,
    dec_v,
    peerdec,
    chin,
    chout,
    enter,
    esend,
    normed,
    atc,
    afc,
    aown,
    ays,
    ayr,
    load_sem,
    a2a_s,
    a2a_r,
    yg_s,
    yg_r,
    cg_s,
    cg_r,
    rc_s,
    rc_r,
    ry_s,
    ry_r,
    rt_s,
    rt_r,
    mc_s,
    mc_r,
    my_s,
    my_r,
    rim_s,
    rim_r,
    st_s,
    st_r,
):
    e = lax.axis_index("ep")
    t = lax.axis_index("tp")
    y = lax.div(t, 2)
    c = lax.rem(t, 2)
    NY = T // 2
    bpc = E // CHUNKS
    tok, width = act_v.shape
    S = width // T
    C = out.shape[1]
    M = bpc * C
    rows, channels = x_v.shape
    latent = b_v.shape[1]
    heads = pre_v.shape[0]
    groups = latent // STATE
    members = heads // groups
    wide = members * HEAD_DIM
    taps = kx_v.shape[0]
    half = STATE // 2
    U = wg_v.shape[1]

    pairs = [
        (picks_h, picks_v),
        (coefs_h, coefs_v),
        (act_h, act_v),
        (bgain_h, bgain_v),
        (x_h, x_v),
        (b_h, b_v),
        (c_h, c_v),
        (kx_h, kx_v),
        (kb_h, kb_v),
        (kc_h, kc_v),
        (pre_h, pre_v),
        (extra_h, extra_v),
        (wg_h, wg_v),
        (wu_h, wu_v),
        (wd_h, wd_v),
        (valve_h, valve_v),
        (again_h, again_v),
        (wr_h, wr_v),
    ]
    loads = {}
    for i, (src, dst) in enumerate(pairs):
        loads[i] = pltpu.make_async_copy(src, dst, load_sem.at[i])
        loads[i].start()

    def ep_peer(j):
        return (jnp.bitwise_xor(e, j), t)

    def y_peer(m):
        return (e, jnp.bitwise_xor(y, m) * 2 + c)

    core_peer = (e, y * 2 + 1 - c)

    barrier = pltpu.get_barrier_semaphore()
    peers = [ep_peer(j) for j in range(1, E)] + [y_peer(m) for m in range(1, NY)] + [core_peer]
    for peer in peers:
        pl.semaphore_signal(barrier, inc=1, device_id=peer, device_id_type=MESH)

    sends = []

    def rcopy(src, dst, ssem, rsem, dev):
        return pltpu.make_async_remote_copy(
            src_ref=src,
            dst_ref=dst,
            send_sem=ssem,
            recv_sem=rsem,
            device_id=dev,
            device_id_type=MESH,
        )

    def send(*args):
        copy = rcopy(*args)
        copy.start()
        sends.append(copy)

    def arrive(dst, rsem):
        rcopy(dst, dst, a2a_s.at[0], rsem, core_peer).wait_recv()

    for i in range(4):
        loads[i].wait()
    pick = jnp.bitwise_xor(picks_v[...], e)
    expert = lax.broadcasted_iota(jnp.int32, (E, tok), 0)
    row_i = lax.broadcasted_iota(jnp.int32, (tok, tok), 0)
    col_i = lax.broadcasted_iota(jnp.int32, (tok, tok), 1)
    before = (row_i < col_i).astype(BF16)
    hot0 = (expert == pick[0:1]).astype(F32)
    hot1 = (expert == pick[1:2]).astype(F32)
    cum0 = dot(hot0.astype(BF16), before)
    cum1 = dot(hot1.astype(BF16), before) + jnp.sum(hot0, axis=1, keepdims=True)
    rank0 = jnp.sum(hot0 * cum0, axis=0, keepdims=True)
    rank1 = jnp.sum(hot1 * cum1, axis=0, keepdims=True)
    slot0 = pick[0:1].astype(F32) * float(C) + rank0
    slot1 = pick[1:2].astype(F32) * float(C) + rank1
    stacked = jnp.concatenate(
        [slot0, slot1, coefs_v[...], jnp.zeros((4, tok), F32)], axis=0
    )
    cols_v[...] = stacked.T

    wide_act = act_v[...].astype(F32)
    scale = lax.rsqrt(jnp.mean(wide_act * wide_act, axis=1, keepdims=True) + NORM_EPS)
    nb[...] = (wide_act * scale * bgain_v[...].astype(F32)).astype(BF16)

    def placing(j):
        slot = (lax.broadcasted_iota(jnp.int32, (C, tok), 0) + j * C).astype(F32)
        return ((slot == slot0) | (slot == slot1)).astype(BF16)

    mine = nb[:, pl.ds(pl.multiple_of(t * S, S), S)]
    for j in range(1, E):
        out[j] = dot(placing(j), mine).astype(BF16)
        if j == 1:
            pl.semaphore_wait(barrier, len(peers))
        send(out.at[j], X.at[t, j], a2a_s.at[j], a2a_r.at[j // bpc], ep_peer(j))

    for i in range(4, 12):
        loads[i].wait()
    tail = pl.ds(rows - HALO, HALO)
    rims = [
        (x_v.at[tail], rim.at[:, pl.ds(0, channels)]),
        (b_v.at[tail], rim.at[:, pl.ds(channels, latent)]),
        (c_v.at[tail], rim.at[:, pl.ds(channels + latent, latent)]),
    ]
    following = (jnp.minimum(e + 1, E - 1), t)

    def rim_copy(i):
        return rcopy(rims[i][0], rims[i][1], rim_s.at[i], rim_r.at[i], following)

    @pl.when(e < E - 1)
    def _():
        for i in range(3):
            rim_copy(i).start()

    @pl.when(e == 0)
    def _():
        rim[...] = jnp.zeros(rim.shape, BF16)

    first = placing(0)
    for tt in range(T):
        X[tt, 0] = dot(first, nb[:, tt * S : (tt + 1) * S]).astype(BF16)

    def span(k):
        return pl.ds(1, bpc - 1) if k == 0 else pl.ds(k * bpc, bpc)

    def share(m, cc):
        return jnp.bitwise_xor(y, m) * 2 + cc

    def forward(k):
        if k == 0 and bpc == 1:
            return
        block = X.at[t, span(k)]
        arrive(block, a2a_r.at[k])
        for m in range(1, NY):
            send(block, block, yg_s.at[m, k], yg_r.at[m, k], y_peer(m))
        send(block, block, cg_s.at[0, k], cg_r.at[0, k], core_peer)

    def forward_core(k):
        if k == 0 and bpc == 1:
            return
        for m in range(1, NY):
            block = X.at[share(m, c), span(k)]
            arrive(block, yg_r.at[m, k])
            send(block, block, cg_s.at[m, k], cg_r.at[m, k], core_peer)

    def ready(k):
        if k == 0 and bpc == 1:
            return
        for m in range(NY):
            arrive(X.at[share(m, 1 - c), span(k)], cg_r.at[m, k])

    NT = min(256, U)
    NS = min(256, S)

    def gate_up(k):
        def body(n, carry):
            at = pl.ds(pl.multiple_of(n * NT, NT), NT)
            gate = up = None
            for tt in range(T):
                r = X[tt, k * bpc : (k + 1) * bpc].reshape(M, S)
                deep = slice(tt * S, (tt + 1) * S)
                g = dot(r, wg_v[deep, at])
                u = dot(r, wu_v[deep, at])
                gate = g if gate is None else gate + g
                up = u if up is None else up + u
            hid[:, at] = (silu(gate) * up).astype(BF16)
            return carry

        lax.fori_loop(0, U // NT, body, 0)

    def down(k):
        for core in (1 - c, c):
            for m in list(range(1, NY)) + [0]:
                base = share(m, core) * S
                for n in range(S // NS):
                    at = pl.ds(pl.multiple_of(base + n * NS, NS), NS)
                    part = dot(hid[...], wd_v[:, at])
                    if core is c:
                        own[k, m, :, n * NS : (n + 1) * NS] = part
                    else:
                        tc[k, m, :, n * NS : (n + 1) * NS] = part.astype(BF16)
                if core is not c:
                    send(tc.at[k, m], fc.at[k, m], rc_s.at[m, k], rc_r.at[m, k], core_peer)

    def reduce_core(k):
        for m in list(range(1, NY)) + [0]:
            arrive(fc.at[k, m], rc_r.at[m, k])
            total = own[k, m] + fc[k, m].astype(F32)
            if m == 0:
                own[k, 0] = total
            else:
                ys[k, m] = total.astype(BF16)
                send(ys.at[k, m], yr.at[k, m], ry_s.at[m, k], ry_r.at[m, k], y_peer(m))

    def reduce_y(k):
        total = own[k, 0]
        for m in range(1, NY):
            arrive(yr.at[k, m], ry_r.at[m, k])
            total = total + yr[k, m].astype(F32)
        done = total.astype(BF16).reshape(bpc, C, S)
        for i in range(bpc):
            j = k * bpc + i
            if j == 0:
                ret[0] = done[0]
            else:
                fin[j] = done[i]
                send(fin.at[j], ret.at[j], rt_s.at[j], rt_r.at[k], ep_peer(j))

    def combine(k):
        if not (k == 0 and bpc == 1):
            arrive(ret.at[span(k)], rt_r.at[k])
        block = ret[k * bpc : (k + 1) * bpc].reshape(M, S)
        lane = (lax.broadcasted_iota(jnp.int32, (tok, M), 1) + k * M).astype(F32)
        total = None
        for p in range(TOPK):
            chosen = (lane == cols_v[:, p : p + 1]).astype(BF16)
            term = dot(chosen, block) * cols_v[:, TOPK + p : TOPK + p + 1]
            total = term if total is None else total + term
        if k > 0:
            total = total + acc[...]
        if k < CHUNKS - 1:
            acc[...] = total
        else:
            outb_ref[...] = total.astype(BF16)

    causal = row_i >= col_i

    def conv(ref, k_ref, start, size, rim_start):
        joined[0:HALO, 0:size] = rim[:, rim_start : rim_start + size].astype(F32)
        joined[HALO : HALO + rows, 0:size] = ref[:, start : start + size].astype(F32)
        kernel = k_ref[:, start : start + size].astype(F32)
        total = None
        for j in range(taps):
            at = HALO - taps + 1 + j
            term = kernel[j : j + 1] * joined[at : at + rows, 0:size]
            total = term if total is None else total + term
        return silu(total)

    def column(ref):
        index = lax.broadcasted_iota(jnp.int32, (heads, rows), 0)
        value = jnp.zeros((heads, rows), F32)
        for h in range(heads):
            value = jnp.where(index == h, ref[h], value)
        return value

    z = pre_v[...] + column(offset_s)
    step_t = jnp.maximum(z, 0.0) + jnp.log1p(jnp.exp(-jnp.abs(z)))
    decay_t = -jnp.exp(column(speed_s)) * step_t + extra_v[...]
    tri = causal.astype(F32)
    eye = (row_i == col_i).astype(F32)
    run = dot_last(tri, decay_t, HIGHEST)
    run_t = dot_last(decay_t, tri, HIGHEST)
    step = dot_last(eye, step_t, HIGHEST)
    last = run[rows - 1 : rows]
    to_end = jnp.exp(last - run)
    grown_v[...] = jnp.exp(run)
    lane128 = lax.broadcasted_iota(jnp.int32, (rows, LANES), 1)
    dec_row = widen(jnp.exp(last), 0, heads, 1)
    dec_v[...] = jnp.broadcast_to(dec_row, dec_v.shape)

    def ssd(g):
        lead = g * members
        cols = slice(g * wide, (g + 1) * wide)
        xc = conv(x_v, kx_v, g * wide, wide, g * wide)
        bb = conv(b_v, kb_v, g * STATE, STATE, channels + g * STATE).astype(BF16)
        cc = conv(c_v, kc_v, g * STATE, STATE, channels + latent + g * STATE).astype(BF16)
        cc_v[:, g * STATE : (g + 1) * STATE] = cc
        xs = xc * widen(step, lead, members, rows)
        xs16 = xs.astype(BF16)
        scores = dot_last(cc, bb)
        scores = jnp.where(causal, scores, 0.0)
        inside = []
        skip = []
        for pair in range(0, members, 2):
            x_pair = xs16[:, pair * HEAD_DIM : (pair + 2) * HEAD_DIM]
            both = []
            for h in (lead + pair, lead + pair + 1):
                gap = jnp.minimum(run[:, h : h + 1] - run_t[h : h + 1, :], 0.0)
                weights = (jnp.exp(gap) * scores).astype(BF16)
                both.append(dot(weights, x_pair))
            inside.append(jnp.where(lane128 < HEAD_DIM, both[0], both[1]))
            h = lead + pair
            skip.append(jnp.where(lane128 < HEAD_DIM, bypass_s[h], bypass_s[h + 1]))
        ybuf[:, cols] = jnp.concatenate(inside, axis=1) + xc * jnp.concatenate(skip, axis=1)
        x_end = (xs * widen(to_end, lead, members, rows)).astype(BF16)
        state[:, cols] = lax.dot_general(
            bb, x_end, (((0,), (0,)), ((), ())), preferred_element_type=F32
        )

    side = lax.rem(e, 2)
    group = lax.div(e, 2)
    pairs_count = E // 2

    def state_exchange():
        st16[0] = state[0:half].astype(BF16)
        st16[1] = state[half:STATE].astype(BF16)
        send(st16.at[1 - side], peerst, st_s.at[0], st_r.at[0], ep_peer(1))
        send(dec_v, peerdec, st_s.at[1], st_r.at[1], ep_peer(1))

    behind = (jnp.maximum(e - 2, 0), t)
    ahead = (jnp.minimum(e + 2, E - 1), t)

    def chain(low, high):
        @pl.when((group >= low) & (group < high))
        def _():
            arrive(peerst, st_r.at[0])
            arrive(peerdec, st_r.at[1])
            own_half = st16[side].astype(F32)
            other = peerst[...].astype(F32)
            own_dec = dec_v[0:1]
            other_dec = peerdec[0:1]
            left = side == 0
            s0 = jnp.where(left, own_half, other)
            s1 = jnp.where(left, other, own_half)
            d0 = jnp.where(left, own_dec, other_dec)
            d1 = jnp.where(left, other_dec, own_dec)

            @pl.when(group > 0)
            def _():
                arrive(chin, st_r.at[2])

            @pl.when(group == 0)
            def _():
                chin[...] = jnp.zeros(chin.shape, BF16)

            e0 = chin[...].astype(F32)
            e1 = e0 * d0 + s0

            @pl.when(group < pairs_count - 1)
            def _():
                chout[...] = (e1 * d1 + s1).astype(BF16)
                rcopy(chout, chin, st_s.at[2], st_r.at[2], ahead).start()

            enter[side] = jnp.where(left, e0, e1).astype(BF16)
            esend[...] = jnp.where(left, e1, e0).astype(BF16)
            rcopy(esend, enter.at[side], st_s.at[3], st_r.at[3], ep_peer(1)).start()

    def gate_norm():
        arrive(enter.at[1 - side], st_r.at[3])
        entered = enter[...].reshape(STATE, channels)
        for g in range(groups):
            cols = slice(g * wide, (g + 1) * wide)
            carried = dot(cc_v[:, g * STATE : (g + 1) * STATE], entered[:, cols])
            ssd_out = ybuf[:, cols] + carried * widen(grown_v[...], g * members, members, rows)
            gated = ssd_out * silu(valve_v[:, cols].astype(F32))
            norm = lax.rsqrt(jnp.mean(gated * gated, axis=1, keepdims=True) + NORM_EPS)
            normed[:, cols] = (gated * norm * again_v[:, cols].astype(F32)).astype(BF16)

    width_a = wr_v.shape[1]
    NA = min(512, width_a)
    R = rows // T

    def project():
        for n in range(width_a // NA):
            part = dot(normed[...], wr_v[:, n * NA : (n + 1) * NA])
            for yy in range(NY):
                m = jnp.bitwise_xor(y, yy)
                low = part[(yy * 2) * R : (yy * 2 + 1) * R]
                high = part[(yy * 2 + 1) * R : (yy * 2 + 2) * R]
                aown[m, :, n * NA : (n + 1) * NA] = jnp.where(c == 0, low, high)
                atc[m, :, n * NA : (n + 1) * NA] = jnp.where(c == 0, high, low).astype(BF16)
        for m in list(range(1, NY)) + [0]:
            send(atc.at[m], afc.at[m], mc_s.at[m], mc_r.at[m], core_peer)

    def mix_core():
        for m in list(range(1, NY)) + [0]:
            arrive(afc.at[m], mc_r.at[m])
            total = aown[m] + afc[m].astype(F32)
            if m == 0:
                aown[0] = total
            else:
                ays[m] = total.astype(BF16)
                send(ays.at[m], ayr.at[m], my_s.at[m], my_r.at[m], y_peer(m))

    def mix_y():
        total = aown[0]
        for m in range(1, NY):
            arrive(ayr.at[m], my_r.at[m])
            total = total + ayr[m].astype(F32)
        outa_ref[...] = total.astype(BF16)

    @pl.when(e > 0)
    def _():
        for i in range(3):
            arrive(rims[i][1], rim_r.at[i])

    for g in range(groups):
        ssd(g)
        if g == 0:
            forward(0)
        if g == 1:
            forward_core(0)
            forward(1)
    if groups < 2:
        forward_core(0)
        forward(1)
    state_exchange()
    ready(0)
    for i in (12, 13, 14):
        loads[i].wait()
    bounds = [round(i * pairs_count / 4) for i in range(5)]
    gate_up(0)
    forward_core(1)
    forward(2)
    chain(bounds[0], bounds[1])
    down(0)
    ready(1)
    gate_up(1)
    chain(bounds[1], bounds[2])
    reduce_core(0)
    forward_core(2)
    forward(3)
    down(1)
    reduce_y(0)
    chain(bounds[2], bounds[3])
    ready(2)
    gate_up(2)
    reduce_core(1)
    forward_core(3)
    down(2)
    chain(bounds[3], bounds[4])
    reduce_y(1)
    combine(0)
    ready(3)
    gate_up(3)
    reduce_core(2)
    down(3)
    for i in (15, 16, 17):
        loads[i].wait()
    gate_norm()
    reduce_y(2)
    reduce_core(3)
    project()
    combine(1)
    mix_core()
    reduce_y(3)
    combine(2)
    mix_y()
    combine(3)

    for copy in sends:
        copy.wait_send()

    @pl.when(e < E - 1)
    def _():
        for i in range(3):
            rim_copy(i).wait_send()

    @pl.when(group < pairs_count - 1)
    def _():
        rcopy(chout, chin, st_s.at[2], st_r.at[2], ahead).wait_send()

    rcopy(esend, enter.at[side], st_s.at[3], st_r.at[3], ep_peer(1)).wait_send()


def local(
    blender_incoming_features,
    entry_latent_matrix,
    exit_latent_matrix,
    unactivated_valve,
    presoftplus_strides,
    extra_attenuation,
    incoming_feature_kernel,
    entry_latent_kernel,
    exit_latent_kernel,
    stride_offset_vector,
    attenuation_speed_exponent,
    bypass_coef_vector,
    cluster_rescale_coefs,
    blender_result_matrix,
    latter_microbatch_activations,
    specialist_rescale_coefs,
    specialist_valve_matrix,
    specialist_expand_matrix,
    specialist_contract_matrix,
    specialist_picks,
    selected_specialist_coefs,
):
    E = lax.axis_size("ep")
    T = lax.axis_size("tp")
    NY = T // 2
    rows, channels = blender_incoming_features.shape
    latent = entry_latent_matrix.shape[1]
    heads = presoftplus_strides.shape[1]
    taps = incoming_feature_kernel.shape[0]
    wide = channels // (latent // STATE)
    half = STATE // 2
    tok, width = latter_microbatch_activations.shape
    S = width // T
    C = 3 * tok * TOPK // (2 * E)
    bpc = E // CHUNKS
    M = bpc * C
    wg, wu, wd = specialist_valve_matrix[0], specialist_expand_matrix[0], specialist_contract_matrix[0]
    U = wg.shape[1]
    width_a = blender_result_matrix.shape[1]
    R = rows // T
    far = [
        specialist_picks.T,
        selected_specialist_coefs.T,
        latter_microbatch_activations,
        specialist_rescale_coefs[None, :],
        blender_incoming_features,
        entry_latent_matrix,
        exit_latent_matrix,
        incoming_feature_kernel,
        entry_latent_kernel,
        exit_latent_kernel,
        presoftplus_strides.T,
        extra_attenuation.T,
        unactivated_valve,
        cluster_rescale_coefs[None, :],
        wg,
        wu,
        wd,
        blender_result_matrix,
    ]
    near = [stride_offset_vector, attenuation_speed_exponent, bypass_coef_vector]
    landing = [pltpu.VMEM(a.shape, a.dtype) for a in far]
    dma = pltpu.SemaphoreType.DMA
    vmem = pltpu.VMEM
    return pl.pallas_call(
        functools.partial(layer_kernel, E, T),
        in_specs=[pl.BlockSpec(memory_space=pl.ANY)] * len(far)
        + [pl.BlockSpec(memory_space=pltpu.SMEM)] * len(near),
        out_specs=[pl.BlockSpec(memory_space=pltpu.VMEM)] * 2,
        out_shape=[
            jax.ShapeDtypeStruct((R, width_a), BF16),
            jax.ShapeDtypeStruct((tok, S), BF16),
        ],
        scratch_shapes=landing
        + [
            vmem((tok, width), BF16),
            vmem((E, C, S), BF16),
            vmem((T, E, C, S), BF16),
            vmem((M, U), BF16),
            vmem((CHUNKS, NY, M, S), BF16),
            vmem((CHUNKS, NY, M, S), BF16),
            vmem((CHUNKS, NY, M, S), F32),
            vmem((CHUNKS, NY, M, S), BF16),
            vmem((CHUNKS, NY, M, S), BF16),
            vmem((E, C, S), BF16),
            vmem((E, C, S), BF16),
            vmem((tok, S), F32),
            vmem((tok, 8), F32),
            vmem((HALO, channels + 2 * latent), BF16),
            vmem((rows + HALO, wide), F32),
            vmem((rows, channels), F32),
            vmem((rows, latent), BF16),
            vmem((rows, heads), F32),
            vmem((STATE, channels), F32),
            vmem((2, half, channels), BF16),
            vmem((half, channels), BF16),
            vmem((8, channels), F32),
            vmem((8, channels), F32),
            vmem((half, channels), BF16),
            vmem((half, channels), BF16),
            vmem((2, half, channels), BF16),
            vmem((half, channels), BF16),
            vmem((rows, channels), BF16),
            vmem((NY, R, width_a), BF16),
            vmem((NY, R, width_a), BF16),
            vmem((NY, R, width_a), F32),
            vmem((NY, R, width_a), BF16),
            vmem((NY, R, width_a), BF16),
            dma((len(far),)),
            dma((E,)),
            dma((CHUNKS,)),
            dma((NY, CHUNKS)),
            dma((NY, CHUNKS)),
            dma((NY, CHUNKS)),
            dma((NY, CHUNKS)),
            dma((NY, CHUNKS)),
            dma((NY, CHUNKS)),
            dma((NY, CHUNKS)),
            dma((NY, CHUNKS)),
            dma((E,)),
            dma((CHUNKS,)),
            dma((NY,)),
            dma((NY,)),
            dma((NY,)),
            dma((NY,)),
            dma((3,)),
            dma((3,)),
            dma((4,)),
            dma((4,)),
        ],
        compiler_params=pltpu.CompilerParams(
            collective_id=0, has_side_effects=True, vmem_limit_bytes=60 * 1024 * 1024
        ),
        name="layer",
    )(*far, *near)


def solution(mesh):
    in_specs = (
        P("ep", "tp"),
        P("ep", "tp"),
        P("ep", "tp"),
        P("ep", "tp"),
        P("ep", "tp"),
        P("ep", "tp"),
        P(None, "tp"),
        P(None, "tp"),
        P(None, "tp"),
        P("tp"),
        P("tp"),
        P("tp"),
        P("tp"),
        P("tp", None),
        P("ep", None),
        P(),
        P("ep", None, "tp"),
        P("ep", None, "tp"),
        P("ep", "tp", None),
        P("ep", None),
        P("ep", None),
    )
    out_specs = (P(("ep", "tp"), None), P("ep", "tp"))
    return jax.shard_map(local, mesh=mesh, in_specs=in_specs, out_specs=out_specs, check_vma=False)
```

time: 169 us -> 84.3 us (0.50)
  waiting for transfers between devices: 50 us -> 0 us
  Pallas kernels: 35.7 us -> 77.5 us
  blocking collectives: 34.5 us -> 0 us
  starting transfers between devices: 19.5 us -> 0 us
  between operations: 14 us -> 0.64 us
  other arithmetic: 3.63 us -> 0 us
  matrix products: 2.95 us -> 0 us
  local copies, waits for them, and re-layouts: 7.76 us -> 5.91 us
    pallas_call x5 -> x1, Pallas kernels: 35.7 us -> 77.5 us  [local(): pl.pallas_call(functools.partial(layer_kernel, E, T), in_specs=[pl.BlockS...]
    all_to_all x2 -> x0, blocking collectives: 34.5 us -> none  [local(): lax.all_to_all(outgoing[:, :, k * size:(k + 1) * size], 'ep', split_axis=...]
    all_to_all x4 -> x0, waiting for transfers between devices: 30.5 us -> none  [the longest x2 12.7 us: local(): lax.all_to_all(summed, 'ep', split_axis=0, concat_axis=0, tiled=True)]
    reduce_scatter x3 -> x0, waiting for transfers between devices: 19.4 us -> none  [the longest x2 10.3 us: local(): lax.psum_scatter(partials[k], 'tp', scatter_dimension=0, tiled=False)]
    all_to_all x4 -> x0, starting transfers between devices: 16.3 us -> none  [the longest x2 7.84 us: local(): lax.all_to_all(summed, 'ep', split_axis=0, concat_axis=0, tiled=True)]
    unnamed x21 -> x2, local copies, waits for them, and re-layouts: 6.71 us -> 3.34 us
    ppermute x1 -> x0, starting transfers between devices: 3 us -> none  [from_behind(): return lax.ppermute(block, axis, route)]
    dot_general x3 -> x0, matrix products: 2.95 us -> none  [the longest x2 1.54 us: local(): jnp.dot(selecting, returned, preferred_element_type=jnp.float32)]
  transfers between devices with their start and end apart: 10 -> 0, of which waited for: 7 -> 0; matrix products, arithmetic and copies ran while one was open for 2% -> 0% of each run, Pallas kernels for 21% -> 0%
where the time goes in v1:
time: 84.3 us; the launch traced here: 84.1 us
  Pallas kernels  77.5 us (92%)
  local copies, waits for them, and re-layouts  5.91 us (7%)
    pallas_call x1, Pallas kernels, local(): pl.pallas_call(functools.partial(layer_kernel, E, T), in_specs=[pl.BlockS...  77.5 us
    unnamed x2, local copies, waits for them, and re-layouts  3.34 us

profile of v1, /device:TPU:0, one launch (start us, length us, event | category | flops | bytes accessed | tf_op | source)
XLA Modules:
  0.0 84.1 jit_solution(2866845693220612709)
XLA Ops:
  0.6 1.3 %broadcast_in_dim.7.again_h = bf16[1,1024]{1,0:T(2,128)(2,1)} reshape(bf16[1024]{0:T(1024)(128)(2,1)} %param.33) | data formatting | bytes 4096 | tf_op jit(solution)/shard_map/broadcast_in_dim | solution.py:676
  1.9 1.3 %broadcast_in_dim.6.bgain_h = bf16[1,2048]{1,0:T(2,128)(2,1)} reshape(bf16[2048]{0:T(1024)(128)(2,1)} %param.36) | data formatting | bytes 8192 | tf_op jit(solution)/shard_map/broadcast_in_dim | solution.py:666
  3.2 77.5 %layer.1 = (bf16[64,2048]{1,0:T(8,128)(2,1)}, bf16[256,512]{1,0:T(8,128)(2,1)}) custom-call(s32[2,256]{1,0:T(2,128)} %bitcast.12, f32[2,256]{1,0:T(2,128)} %bitcast.13, bf16[256,2048]{1,0:T(8,128)(2,1)} %act_h.1, bf16[1,2048]{1,0:T(2,128)(2,1)} %broadcast_in_dim.6.bgain_h, bf16[256,1024]{1,0:T(8,128)(2,1)} %x_h.1, bf16[256,512]{1,0:T(8,128)(2,1)} %b_h.1, ...), custom_call_target="tpu_custom_call" | custom-call | tf_op jit(solution)/shard_map/layer/pallas_call | solution.py:686
  80.7 1.7 %copy.25 = bf16[64,2048]{1,0:T(8,128)(2,1)} copy(bf16[64,2048]{1,0:T(8,128)(2,1)} %get-tuple-element.4) | data formatting | bytes 524288
  82.4 1.7 %copy.26 = bf16[256,512]{1,0:T(8,128)(2,1)} copy(bf16[256,512]{1,0:T(8,128)(2,1)} %get-tuple-element.5) | data formatting | bytes 524288

commit v2 on v1

--- a/solution.py
+++ b/solution.py
@@ -20,7 +20,68 @@
 BF16 = jnp.bfloat16
 HALO = 16
 LANES = 128
-CHUNKS = 4
+UNITS = 8
+GROUPS = ((0, 1), (1, 1), (2, 2), (4, 2), (6, 2))
+SENDING = (2, 3, 5, 1, 4, 6, 7)
+
+ORDER = (
+    ("mp",),
+    ("fw", 0),
+    ("ssd", 0),
+    ("ssd", 1),
+    ("fw", 2),
+    ("ssd", 2),
+    ("ssd", 3),
+    ("rd", 0),
+    ("sx",),
+    ("fc", 0),
+    ("fw", 4),
+    ("lw",),
+    ("gu", 0),
+    ("dn", 0),
+    ("ch", 0),
+    ("fc", 2),
+    ("fc", 1),
+    ("fc", 4),
+    ("fw", 6),
+    ("rd", 4),
+    ("ch", 1),
+    ("fw", 1),
+    ("gu", 4),
+    ("rd", 2),
+    ("dn", 4),
+    ("fc", 6),
+    ("rd", 1),
+    ("rc", 4),
+    ("rd", 6),
+    ("ch", 2),
+    ("gu", 6),
+    ("dn", 6),
+    ("rc", 0),
+    ("ry", 4),
+    ("gu", 1),
+    ("rc", 6),
+    ("ch", 3),
+    ("dn", 1),
+    ("gu", 2),
+    ("dn", 2),
+    ("rc", 1),
+    ("ry", 6),
+    ("lr",),
+    ("gn",),
+    ("rc", 2),
+    ("pj",),
+    ("ry", 1),
+    ("mc",),
+    ("ry", 2),
+    ("cb", 4),
+    ("ry", 0),
+    ("cb", 1),
+    ("cb", 6),
+    ("cb", 0),
+    ("cb", 2),
+    ("my",),
+)
 
 
 def silu(v):
@@ -93,6 +154,7 @@
     wr_v,
     nb,
     out,
+    out1,
     X,
     hid,
     tc,
@@ -127,6 +189,7 @@
     load_sem,
     a2a_s,
     a2a_r,
+    a2a_r1,
     yg_s,
     yg_r,
     cg_s,
@@ -151,11 +214,15 @@
     y = lax.div(t, 2)
     c = lax.rem(t, 2)
     NY = T // 2
-    bpc = E // CHUNKS
+    b = E // UNITS
+    blocks = {first: (first * b, count * b) for first, count in GROUPS}
+    chunk_of = {}
+    for k, (j0, n) in blocks.items():
+        for j in range(j0, j0 + n):
+            chunk_of[j] = k
     tok, width = act_v.shape
     S = width // T
     C = out.shape[1]
-    M = bpc * C
     rows, channels = x_v.shape
     latent = b_v.shape[1]
     heads = pre_v.shape[0]
@@ -222,10 +289,11 @@
         sends.append(copy)
 
     def arrive(dst, rsem):
-        rcopy(dst, dst, a2a_s.at[0], rsem, core_peer).wait_recv()
-
-    for i in range(4):
-        loads[i].wait()
+        rcopy(dst, dst, a2a_s.at[0, 0], rsem, core_peer).wait_recv()
+
+    with jax.named_scope("load_b"):
+        for i in range(4):
+            loads[i].wait()
     pick = jnp.bitwise_xor(picks_v[...], e)
     expert = lax.broadcasted_iota(jnp.int32, (E, tok), 0)
     row_i = lax.broadcasted_iota(jnp.int32, (tok, tok), 0)
@@ -246,21 +314,17 @@
 
     wide_act = act_v[...].astype(F32)
     scale = lax.rsqrt(jnp.mean(wide_act * wide_act, axis=1, keepdims=True) + NORM_EPS)
-    nb[...] = (wide_act * scale * bgain_v[...].astype(F32)).astype(BF16)
+    nb[...] = (wide_act * scale * bgain_v[...].astype(F32)[None, :]).astype(BF16)
 
     def placing(j):
         slot = (lax.broadcasted_iota(jnp.int32, (C, tok), 0) + j * C).astype(F32)
         return ((slot == slot0) | (slot == slot1)).astype(BF16)
 
-    mine = nb[:, pl.ds(pl.multiple_of(t * S, S), S)]
-    for j in range(1, E):
-        out[j] = dot(placing(j), mine).astype(BF16)
-        if j == 1:
-            pl.semaphore_wait(barrier, len(peers))
-        send(out.at[j], X.at[t, j], a2a_s.at[j], a2a_r.at[j // bpc], ep_peer(j))
-
-    for i in range(4, 12):
-        loads[i].wait()
+    with jax.named_scope("load_a"):
+        for i in range(4, 12):
+            loads[i].wait()
+    with jax.named_scope("barrier"):
+        pl.semaphore_wait(barrier, len(peers))
     tail = pl.ds(rows - HALO, HALO)
     rims = [
         (x_v.at[tail], rim.at[:, pl.ds(0, channels)]),
@@ -281,109 +345,144 @@
     def _():
         rim[...] = jnp.zeros(rim.shape, BF16)
 
+    def normed_share(tt):
+        return nb[:, pl.ds(pl.multiple_of(tt * S, S), S)]
+
+    def share(m, cc):
+        return jnp.bitwise_xor(y, m) * 2 + cc
+
+    mine = normed_share(t)
+    leaving = [j for unit in (0,) + SENDING for j in range(unit * b, unit * b + b) if j > 0]
+    for j in leaving:
+        k = chunk_of[j]
+        placed = placing(j)
+        out[j] = dot(placed, mine).astype(BF16)
+        send(out.at[j], X.at[t, j], a2a_s.at[0, j], a2a_r.at[k], ep_peer(j))
+        if k == 1:
+            for m in range(1, NY):
+                other = out1.at[m, j - b]
+                other[...] = dot(placed, normed_share(share(m, c))).astype(BF16)
+                send(other, X.at[share(m, c), j], a2a_s.at[m, j], a2a_r1.at[m], ep_peer(j))
+
     first = placing(0)
     for tt in range(T):
         X[tt, 0] = dot(first, nb[:, tt * S : (tt + 1) * S]).astype(BF16)
 
     def span(k):
-        return pl.ds(1, bpc - 1) if k == 0 else pl.ds(k * bpc, bpc)
-
-    def share(m, cc):
-        return jnp.bitwise_xor(y, m) * 2 + cc
+        j0, n = blocks[k]
+        return pl.ds(1, n - 1) if k == 0 else pl.ds(j0, n)
+
+    def local_only(k):
+        return blocks[k][0] == 0 and blocks[k][1] == 1
 
     def forward(k):
-        if k == 0 and bpc == 1:
+        if local_only(k):
             return
         block = X.at[t, span(k)]
         arrive(block, a2a_r.at[k])
-        for m in range(1, NY):
-            send(block, block, yg_s.at[m, k], yg_r.at[m, k], y_peer(m))
+        if k != 1:
+            for m in range(1, NY):
+                send(block, block, yg_s.at[m, k], yg_r.at[m, k], y_peer(m))
         send(block, block, cg_s.at[0, k], cg_r.at[0, k], core_peer)
 
     def forward_core(k):
-        if k == 0 and bpc == 1:
+        if local_only(k):
             return
         for m in range(1, NY):
             block = X.at[share(m, c), span(k)]
-            arrive(block, yg_r.at[m, k])
+            arrive(block, a2a_r1.at[m] if k == 1 else yg_r.at[m, k])
             send(block, block, cg_s.at[m, k], cg_r.at[m, k], core_peer)
 
     def ready(k):
-        if k == 0 and bpc == 1:
+        if local_only(k):
             return
         for m in range(NY):
             arrive(X.at[share(m, 1 - c), span(k)], cg_r.at[m, k])
 
-    NT = min(256, U)
+    NT = min(512, U)
     NS = min(256, S)
 
+    def span_rows(k):
+        j0, n = blocks[k]
+        return pl.ds(j0 * C, n * C)
+
     def gate_up(k):
-        def body(n, carry):
-            at = pl.ds(pl.multiple_of(n * NT, NT), NT)
+        j0, n = blocks[k]
+
+        def body(i, carry):
+            at = pl.ds(pl.multiple_of(i * NT, NT), NT)
             gate = up = None
             for tt in range(T):
-                r = X[tt, k * bpc : (k + 1) * bpc].reshape(M, S)
+                r = X[tt, j0 : j0 + n].reshape(n * C, S)
                 deep = slice(tt * S, (tt + 1) * S)
                 g = dot(r, wg_v[deep, at])
                 u = dot(r, wu_v[deep, at])
                 gate = g if gate is None else gate + g
                 up = u if up is None else up + u
-            hid[:, at] = (silu(gate) * up).astype(BF16)
+            hid[0 : n * C, at] = (silu(gate) * up).astype(BF16)
             return carry
 
         lax.fori_loop(0, U // NT, body, 0)
 
     def down(k):
-        for core in (1 - c, c):
+        rs = span_rows(k)
+        size = blocks[k][1] * C
+        for mine_side in (False, True):
+            core = c if mine_side else 1 - c
             for m in list(range(1, NY)) + [0]:
                 base = share(m, core) * S
                 for n in range(S // NS):
                     at = pl.ds(pl.multiple_of(base + n * NS, NS), NS)
-                    part = dot(hid[...], wd_v[:, at])
-                    if core is c:
-                        own[k, m, :, n * NS : (n + 1) * NS] = part
+                    part = dot(hid[0:size], wd_v[:, at])
+                    if mine_side:
+                        own[m, rs, n * NS : (n + 1) * NS] = part
                     else:
-                        tc[k, m, :, n * NS : (n + 1) * NS] = part.astype(BF16)
-                if core is not c:
-                    send(tc.at[k, m], fc.at[k, m], rc_s.at[m, k], rc_r.at[m, k], core_peer)
+                        tc[m, rs, n * NS : (n + 1) * NS] = part.astype(BF16)
+                if not mine_side:
+                    send(tc.at[m, rs], fc.at[m, rs], rc_s.at[m, k], rc_r.at[m, k], core_peer)
 
     def reduce_core(k):
+        rs = span_rows(k)
         for m in list(range(1, NY)) + [0]:
-            arrive(fc.at[k, m], rc_r.at[m, k])
-            total = own[k, m] + fc[k, m].astype(F32)
+            arrive(fc.at[m, rs], rc_r.at[m, k])
+            total = own[m, rs] + fc[m, rs].astype(F32)
             if m == 0:
-                own[k, 0] = total
+                own[0, rs] = total
             else:
-                ys[k, m] = total.astype(BF16)
-                send(ys.at[k, m], yr.at[k, m], ry_s.at[m, k], ry_r.at[m, k], y_peer(m))
+                ys[m, rs] = total.astype(BF16)
+                send(ys.at[m, rs], yr.at[m, rs], ry_s.at[m, k], ry_r.at[m, k], y_peer(m))
 
     def reduce_y(k):
-        total = own[k, 0]
+        j0, n = blocks[k]
+        rs = span_rows(k)
+        total = own[0, rs]
         for m in range(1, NY):
-            arrive(yr.at[k, m], ry_r.at[m, k])
-            total = total + yr[k, m].astype(F32)
-        done = total.astype(BF16).reshape(bpc, C, S)
-        for i in range(bpc):
-            j = k * bpc + i
+            arrive(yr.at[m, rs], ry_r.at[m, k])
+            total = total + yr[m, rs].astype(F32)
+        done = total.astype(BF16).reshape(n, C, S)
+        for i in range(n):
+            j = j0 + i
             if j == 0:
                 ret[0] = done[0]
             else:
                 fin[j] = done[i]
                 send(fin.at[j], ret.at[j], rt_s.at[j], rt_r.at[k], ep_peer(j))
 
-    def combine(k):
-        if not (k == 0 and bpc == 1):
+    def combine(k, place):
+        if not local_only(k):
             arrive(ret.at[span(k)], rt_r.at[k])
-        block = ret[k * bpc : (k + 1) * bpc].reshape(M, S)
-        lane = (lax.broadcasted_iota(jnp.int32, (tok, M), 1) + k * M).astype(F32)
+        j0, n = blocks[k]
+        size = n * C
+        block = ret[j0 : j0 + n].reshape(size, S)
+        lane = (lax.broadcasted_iota(jnp.int32, (tok, size), 1) + j0 * C).astype(F32)
         total = None
         for p in range(TOPK):
             chosen = (lane == cols_v[:, p : p + 1]).astype(BF16)
             term = dot(chosen, block) * cols_v[:, TOPK + p : TOPK + p + 1]
             total = term if total is None else total + term
-        if k > 0:
+        if place != "first":
             total = total + acc[...]
-        if k < CHUNKS - 1:
+        if place != "last":
             acc[...] = total
         else:
             outb_ref[...] = total.astype(BF16)
@@ -408,22 +507,32 @@
             value = jnp.where(index == h, ref[h], value)
         return value
 
-    z = pre_v[...] + column(offset_s)
-    step_t = jnp.maximum(z, 0.0) + jnp.log1p(jnp.exp(-jnp.abs(z)))
-    decay_t = -jnp.exp(column(speed_s)) * step_t + extra_v[...]
-    tri = causal.astype(F32)
-    eye = (row_i == col_i).astype(F32)
-    run = dot_last(tri, decay_t, HIGHEST)
-    run_t = dot_last(decay_t, tri, HIGHEST)
-    step = dot_last(eye, step_t, HIGHEST)
-    last = run[rows - 1 : rows]
-    to_end = jnp.exp(last - run)
-    grown_v[...] = jnp.exp(run)
+    mix = {}
     lane128 = lax.broadcasted_iota(jnp.int32, (rows, LANES), 1)
-    dec_row = widen(jnp.exp(last), 0, heads, 1)
-    dec_v[...] = jnp.broadcast_to(dec_row, dec_v.shape)
+
+    def mix_prepare():
+        z = pre_v[...] + column(offset_s)
+        step_t = jnp.maximum(z, 0.0) + jnp.log1p(jnp.exp(-jnp.abs(z)))
+        decay_t = -jnp.exp(column(speed_s)) * step_t + extra_v[...]
+        tri = causal.astype(F32)
+        eye = (row_i == col_i).astype(F32)
+        run = dot_last(tri, decay_t, HIGHEST)
+        last = run[rows - 1 : rows]
+        grown_v[...] = jnp.exp(run)
+        dec_row = widen(jnp.exp(last), 0, heads, 1)
+        dec_v[...] = jnp.broadcast_to(dec_row, dec_v.shape)
+        mix["run"] = run
+        mix["run_t"] = dot_last(decay_t, tri, HIGHEST)
+        mix["step"] = dot_last(eye, step_t, HIGHEST)
+        mix["to_end"] = jnp.exp(last - run)
+
+        @pl.when(e > 0)
+        def _():
+            for i in range(3):
+                arrive(rims[i][1], rim_r.at[i])
 
     def ssd(g):
+        run, run_t, step, to_end = (mix[n] for n in ("run", "run_t", "step", "to_end"))
         lead = g * members
         cols = slice(g * wide, (g + 1) * wide)
         xc = conv(x_v, kx_v, g * wide, wide, g * wide)
@@ -509,7 +618,7 @@
             ssd_out = ybuf[:, cols] + carried * widen(grown_v[...], g * members, members, rows)
             gated = ssd_out * silu(valve_v[:, cols].astype(F32))
             norm = lax.rsqrt(jnp.mean(gated * gated, axis=1, keepdims=True) + NORM_EPS)
-            normed[:, cols] = (gated * norm * again_v[:, cols].astype(F32)).astype(BF16)
+            normed[:, cols] = (gated * norm * again_v[cols].astype(F32)[None, :]).astype(BF16)
 
     width_a = wr_v.shape[1]
     NA = min(512, width_a)
@@ -544,67 +653,56 @@
             total = total + ayr[m].astype(F32)
         outa_ref[...] = total.astype(BF16)
 
-    @pl.when(e > 0)
-    def _():
-        for i in range(3):
-            arrive(rims[i][1], rim_r.at[i])
-
-    for g in range(groups):
-        ssd(g)
-        if g == 0:
-            forward(0)
-        if g == 1:
-            forward_core(0)
-            forward(1)
-    if groups < 2:
-        forward_core(0)
-        forward(1)
-    state_exchange()
-    ready(0)
-    for i in (12, 13, 14):
-        loads[i].wait()
     bounds = [round(i * pairs_count / 4) for i in range(5)]
-    gate_up(0)
-    forward_core(1)
-    forward(2)
-    chain(bounds[0], bounds[1])
-    down(0)
-    ready(1)
-    gate_up(1)
-    chain(bounds[1], bounds[2])
-    reduce_core(0)
-    forward_core(2)
-    forward(3)
-    down(1)
-    reduce_y(0)
-    chain(bounds[2], bounds[3])
-    ready(2)
-    gate_up(2)
-    reduce_core(1)
-    forward_core(3)
-    down(2)
-    chain(bounds[3], bounds[4])
-    reduce_y(1)
-    combine(0)
-    ready(3)
-    gate_up(3)
-    reduce_core(2)
-    down(3)
-    for i in (15, 16, 17):
-        loads[i].wait()
-    gate_norm()
-    reduce_y(2)
-    reduce_core(3)
-    project()
-    combine(1)
-    mix_core()
-    reduce_y(3)
-    combine(2)
-    mix_y()
-    combine(3)
-
-    for copy in sends:
-        copy.wait_send()
+    seen = []
+
+    def load_weights():
+        for i in (12, 13, 14):
+            loads[i].wait()
+
+    def load_rest():
+        for i in (15, 16, 17):
+            loads[i].wait()
+
+    def ssd_part(i):
+        for g in range(i * groups // 4, (i + 1) * groups // 4):
+            ssd(g)
+
+    def chain_part(i):
+        chain(bounds[i], bounds[i + 1])
+
+    def combine_part(k):
+        seen.append(k)
+        place = "first" if len(seen) == 1 else "last" if len(seen) == len(blocks) else "add"
+        combine(k, place)
+
+    steps = {
+        "fw": forward,
+        "fc": forward_core,
+        "rd": ready,
+        "gu": gate_up,
+        "dn": down,
+        "rc": reduce_core,
+        "ry": reduce_y,
+        "cb": combine_part,
+        "mp": mix_prepare,
+        "ssd": ssd_part,
+        "sx": state_exchange,
+        "ch": chain_part,
+        "lw": load_weights,
+        "lr": load_rest,
+        "gn": gate_norm,
+        "pj": project,
+        "mc": mix_core,
+        "my": mix_y,
+    }
+    for name, *which in ORDER:
+        with jax.named_scope(name + "".join(str(i) for i in which)):
+            steps[name](*which)
+
+    with jax.named_scope("drain"):
+        for copy in sends:
+            copy.wait_send()
 
     @pl.when(e < E - 1)
     def _():
@@ -653,8 +751,7 @@
     tok, width = latter_microbatch_activations.shape
     S = width // T
     C = 3 * tok * TOPK // (2 * E)
-    bpc = E // CHUNKS
-    M = bpc * C
+    b = E // UNITS
     wg, wu, wd = specialist_valve_matrix[0], specialist_expand_matrix[0], specialist_contract_matrix[0]
     U = wg.shape[1]
     width_a = blender_result_matrix.shape[1]
@@ -663,7 +760,7 @@
         specialist_picks.T,
         selected_specialist_coefs.T,
         latter_microbatch_activations,
-        specialist_rescale_coefs[None, :],
+        specialist_rescale_coefs,
         blender_incoming_features,
         entry_latent_matrix,
         exit_latent_matrix,
@@ -673,7 +770,7 @@
         presoftplus_strides.T,
         extra_attenuation.T,
         unactivated_valve,
-        cluster_rescale_coefs[None, :],
+        cluster_rescale_coefs,
         wg,
         wu,
         wd,
@@ -688,21 +785,19 @@
         in_specs=[pl.BlockSpec(memory_space=pl.ANY)] * len(far)
         + [pl.BlockSpec(memory_space=pltpu.SMEM)] * len(near),
         out_specs=[pl.BlockSpec(memory_space=pltpu.VMEM)] * 2,
-        out_shape=[
-            jax.ShapeDtypeStruct((R, width_a), BF16),
-            jax.ShapeDtypeStruct((tok, S), BF16),
-        ],
+        out_shape=[pltpu.VMEM((R, width_a), BF16), pltpu.VMEM((tok, S), BF16)],
         scratch_shapes=landing
         + [
             vmem((tok, width), BF16),
             vmem((E, C, S), BF16),
+            vmem((NY, b, C, S), BF16),
             vmem((T, E, C, S), BF16),
-            vmem((M, U), BF16),
-            vmem((CHUNKS, NY, M, S), BF16),
-            vmem((CHUNKS, NY, M, S), BF16),
-            vmem((CHUNKS, NY, M, S), F32),
-            vmem((CHUNKS, NY, M, S), BF16),
-            vmem((CHUNKS, NY, M, S), BF16),
+            vmem((max(n for _, n in GROUPS) * b * C, U), BF16),
+            vmem((NY, E * C, S), BF16),
+            vmem((NY, E * C, S), BF16),
+            vmem((NY, E * C, S), F32),
+            vmem((NY, E * C, S), BF16),
+            vmem((NY, E * C, S), BF16),
             vmem((E, C, S), BF16),
             vmem((E, C, S), BF16),
             vmem((tok, S), F32),
@@ -728,18 +823,19 @@
             vmem((NY, R, width_a), BF16),
             vmem((NY, R, width_a), BF16),
             dma((len(far),)),
+            dma((NY, E)),
+            dma((UNITS,)),
+            dma((NY,)),
+            dma((NY, UNITS)),
+            dma((NY, UNITS)),
+            dma((NY, UNITS)),
+            dma((NY, UNITS)),
+            dma((NY, UNITS)),
+            dma((NY, UNITS)),
+            dma((NY, UNITS)),
+            dma((NY, UNITS)),
             dma((E,)),
-            dma((CHUNKS,)),
-            dma((NY, CHUNKS)),
-            dma((NY, CHUNKS)),
-            dma((NY, CHUNKS)),
-            dma((NY, CHUNKS)),
-            dma((NY, CHUNKS)),
-            dma((NY, CHUNKS)),
-            dma((NY, CHUNKS)),
-            dma((NY, CHUNKS)),
-            dma((E,)),
-            dma((CHUNKS,)),
+            dma((UNITS,)),
             dma((NY,)),
             dma((NY,)),
             dma((NY,)),

time: 84.3 us -> 64.5 us (0.77)
  Pallas kernels: 77.5 us -> 62.3 us
  local copies, waits for them, and re-layouts: 5.91 us -> 1.41 us
    pallas_call x1, Pallas kernels: 77.5 us -> 62.3 us  [local(): pl.pallas_call(functools.partial(layer_kernel, E, T), in_specs=[pl.BlockS...]
    broadcast_in_dim x2 -> x0, local copies, waits for them, and re-layouts: 2.57 us -> none  [the longest x1 1.29 us: local(): specialist_rescale_coefs[None, :]]
    unnamed x2, local copies, waits for them, and re-layouts: 3.34 us -> 1.41 us
where the time goes in v2:
time: 64.5 us; the launch traced here: 64.3 us
  Pallas kernels  62.3 us (97%)
  local copies, waits for them, and re-layouts  1.41 us (2%)
  between operations  0.65 us (1%)
    pallas_call x1, Pallas kernels, local(): pl.pallas_call(functools.partial(layer_kernel, E, T), in_specs=[pl.BlockS...  62.3 us
    unnamed x2, local copies, waits for them, and re-layouts  1.41 us

profile of v2, /device:TPU:0, one launch (start us, length us, event | category | flops | bytes accessed | tf_op | source)
XLA Modules:
  0.0 64.3 jit_solution(8429754570052865774)
XLA Ops:
  0.6 62.3 %layer.1 = (bf16[64,2048]{1,0:T(8,128)(2,1)S(1)}, bf16[256,512]{1,0:T(8,128)(2,1)S(1)}) custom-call(s32[2,256]{1,0:T(2,128)} %bitcast.12, f32[2,256]{1,0:T(2,128)} %bitcast.13, bf16[256,2048]{1,0:T(8,128)(2,1)} %act_h.1, bf16[2048]{0:T(1024)(128)(2,1)} %bgain_h.1, bf16[256,1024]{1,0:T(8,128)(2,1)} %x_h.1, bf16[256,512]{1,0:T(8,128)(2,1)} %b_h.1, ...), custom_call_target="tpu_custom_call" | custom-call | tf_op jit(solution)/shard_map/layer/pallas_call | solution.py:783
  62.9 0.7 %copy.25 = bf16[64,2048]{1,0:T(8,128)(2,1)} copy(bf16[64,2048]{1,0:T(8,128)(2,1)S(1)} %get-tuple-element.2) | data formatting | bytes 524288
  63.6 0.7 %copy.26 = bf16[256,512]{1,0:T(8,128)(2,1)} copy(bf16[256,512]{1,0:T(8,128)(2,1)S(1)} %get-tuple-element.3) | data formatting | bytes 524288

commit v3 on v2

--- a/solution.py
+++ b/solution.py
@@ -21,66 +21,84 @@
 HALO = 16
 LANES = 128
 UNITS = 8
-GROUPS = ((0, 1), (1, 1), (2, 2), (4, 2), (6, 2))
-SENDING = (2, 3, 5, 1, 4, 6, 7)
+GROUPS = ((0, 1), (1, 1), (2, 2), (4, 1), (5, 1), (6, 1), (7, 1))
+KINDS = ("out", "out1", "y", "core", "tc", "ys", "fin", "rim", "st16", "dec", "chain", "enter", "atc", "ays")
+TWICE = 1
+SENDING = (2, 4, 1, 5, 3, 7, 6)
 
 ORDER = (
+    ("rd", 0),
+    ("lw",),
+    ("gu", 0),
     ("mp",),
-    ("fw", 0),
+    ("fw", 2),
     ("ssd", 0),
+    ("fw", 4),
     ("ssd", 1),
-    ("fw", 2),
+    ("fc", 1),
+    ("fw", 1),
     ("ssd", 2),
     ("ssd", 3),
-    ("rd", 0),
     ("sx",),
-    ("fc", 0),
-    ("fw", 4),
-    ("lw",),
-    ("gu", 0),
+    ("fc", 4),
+    ("rd", 1),
+    ("fw", 3),
     ("dn", 0),
+    ("fw", 5),
+    ("gu", 1),
+    ("rd", 4),
     ("ch", 0),
+    ("rc", 0),
+    ("dn", 1),
+    ("gu", 4),
+    ("rc", 1),
+    ("fc", 5),
+    ("dn", 4),
     ("fc", 2),
-    ("fc", 1),
-    ("fc", 4),
     ("fw", 6),
-    ("rd", 4),
     ("ch", 1),
-    ("fw", 1),
-    ("gu", 4),
+    ("rd", 5),
+    ("fc", 3),
+    ("gu", 5),
+    ("rc", 4),
+    ("dn", 5),
+    ("fw", 7),
     ("rd", 2),
-    ("dn", 4),
+    ("gu", 2),
     ("fc", 6),
-    ("rd", 1),
-    ("rc", 4),
+    ("rc", 5),
+    ("ch", 2),
+    ("ry", 1),
+    ("dn", 2),
     ("rd", 6),
-    ("ch", 2),
+    ("ry", 4),
     ("gu", 6),
     ("dn", 6),
-    ("rc", 0),
-    ("ry", 4),
-    ("gu", 1),
+    ("fc", 7),
+    ("ch", 3),
     ("rc", 6),
-    ("ch", 3),
-    ("dn", 1),
-    ("gu", 2),
-    ("dn", 2),
-    ("rc", 1),
-    ("ry", 6),
+    ("ry", 0),
+    ("ry", 5),
+    ("rc", 2),
+    ("rd", 7),
+    ("gu", 7),
+    ("dn", 7),
     ("lr",),
     ("gn",),
-    ("rc", 2),
+    ("rc", 7),
+    ("ry", 6),
+    ("cb", 1),
     ("pj",),
-    ("ry", 1),
+    ("ry", 2),
+    ("cb", 5),
     ("mc",),
-    ("ry", 2),
-    ("cb", 4),
-    ("ry", 0),
-    ("cb", 1),
+    ("ry", 7),
     ("cb", 6),
     ("cb", 0),
+    ("cb", 4),
     ("cb", 2),
     ("my",),
+    ("cb", 7),
 )
 
 
@@ -187,27 +205,15 @@
     ays,
     ayr,
     load_sem,
-    a2a_s,
-    a2a_r,
-    a2a_r1,
-    yg_s,
-    yg_r,
-    cg_s,
-    cg_r,
-    rc_s,
-    rc_r,
-    ry_s,
-    ry_r,
-    rt_s,
-    rt_r,
-    mc_s,
-    mc_r,
-    my_s,
-    my_r,
-    rim_s,
-    rim_r,
-    st_s,
-    st_r,
+    sent,
+    out_r,
+    y_r,
+    core_r,
+    sum_r,
+    ysum_r,
+    ret_r,
+    once_r,
+    state_r,
 ):
     e = lax.axis_index("ep")
     t = lax.axis_index("tp")
@@ -216,10 +222,7 @@
     NY = T // 2
     b = E // UNITS
     blocks = {first: (first * b, count * b) for first, count in GROUPS}
-    chunk_of = {}
-    for k, (j0, n) in blocks.items():
-        for j in range(j0, j0 + n):
-            chunk_of[j] = k
+    units = {first: range(first, first + count) for first, count in GROUPS}
     tok, width = act_v.shape
     S = width // T
     C = out.shape[1]
@@ -271,8 +274,6 @@
     for peer in peers:
         pl.semaphore_signal(barrier, inc=1, device_id=peer, device_id_type=MESH)
 
-    sends = []
-
     def rcopy(src, dst, ssem, rsem, dev):
         return pltpu.make_async_remote_copy(
             src_ref=src,
@@ -283,13 +284,18 @@
             device_id_type=MESH,
         )
 
-    def send(*args):
-        copy = rcopy(*args)
-        copy.start()
-        sends.append(copy)
+    def send(src, dst, kind, rsem, dev):
+        rcopy(src, dst, sent.at[KINDS.index(kind)], rsem, dev).start()
+
+    def drain(kind, whole):
+        rcopy(whole, whole, sent.at[KINDS.index(kind)], state_r.at[0], core_peer).wait_send()
 
     def arrive(dst, rsem):
-        rcopy(dst, dst, a2a_s.at[0, 0], rsem, core_peer).wait_recv()
+        rcopy(dst, dst, sent.at[0], rsem, core_peer).wait_recv()
+
+    index_of = {k: i for i, k in enumerate(blocks)}
+    others = pl.ds(1, NY - 1)
+    every = pl.ds(0, NY)
 
     with jax.named_scope("load_b"):
         for i in range(4):
@@ -333,13 +339,10 @@
     ]
     following = (jnp.minimum(e + 1, E - 1), t)
 
-    def rim_copy(i):
-        return rcopy(rims[i][0], rims[i][1], rim_s.at[i], rim_r.at[i], following)
-
     @pl.when(e < E - 1)
     def _():
-        for i in range(3):
-            rim_copy(i).start()
+        for src, dst in rims:
+            send(src, dst, "rim", once_r.at[1], following)
 
     @pl.when(e == 0)
     def _():
@@ -354,15 +357,15 @@
     mine = normed_share(t)
     leaving = [j for unit in (0,) + SENDING for j in range(unit * b, unit * b + b) if j > 0]
     for j in leaving:
-        k = chunk_of[j]
+        u = j // b
         placed = placing(j)
         out[j] = dot(placed, mine).astype(BF16)
-        send(out.at[j], X.at[t, j], a2a_s.at[0, j], a2a_r.at[k], ep_peer(j))
-        if k == 1:
+        send(out.at[j], X.at[t, j], "out", out_r.at[u], ep_peer(j))
+        if u == TWICE:
             for m in range(1, NY):
-                other = out1.at[m, j - b]
+                other = out1.at[m, j - TWICE * b]
                 other[...] = dot(placed, normed_share(share(m, c))).astype(BF16)
-                send(other, X.at[share(m, c), j], a2a_s.at[m, j], a2a_r1.at[m], ep_peer(j))
+                send(other, X.at[share(m, c), j], "out1", once_r.at[0], ep_peer(j))
 
     first = placing(0)
     for tt in range(T):
@@ -372,32 +375,33 @@
         j0, n = blocks[k]
         return pl.ds(1, n - 1) if k == 0 else pl.ds(j0, n)
 
+    def unit(u):
+        return pl.ds(1, b - 1) if u == 0 else pl.ds(u * b, b)
+
     def local_only(k):
         return blocks[k][0] == 0 and blocks[k][1] == 1
 
-    def forward(k):
-        if local_only(k):
-            return
-        block = X.at[t, span(k)]
-        arrive(block, a2a_r.at[k])
-        if k != 1:
+    def forward(u):
+        block = X.at[t, unit(u)]
+        arrive(block, out_r.at[u])
+        if u != TWICE:
             for m in range(1, NY):
-                send(block, block, yg_s.at[m, k], yg_r.at[m, k], y_peer(m))
-        send(block, block, cg_s.at[0, k], cg_r.at[0, k], core_peer)
-
-    def forward_core(k):
-        if local_only(k):
-            return
+                send(block, block, "y", y_r.at[u], y_peer(m))
+        send(block, block, "core", core_r.at[u], core_peer)
+
+    def forward_core(u):
+        arrive(X.at[pl.ds(0, NY - 1), unit(u)], once_r.at[0] if u == TWICE else y_r.at[u])
         for m in range(1, NY):
-            block = X.at[share(m, c), span(k)]
-            arrive(block, a2a_r1.at[m] if k == 1 else yg_r.at[m, k])
-            send(block, block, cg_s.at[m, k], cg_r.at[m, k], core_peer)
+            block = X.at[share(m, c), unit(u)]
+            send(block, block, "core", core_r.at[u], core_peer)
 
     def ready(k):
-        if local_only(k):
-            return
-        for m in range(NY):
-            arrive(X.at[share(m, 1 - c), span(k)], cg_r.at[m, k])
+        if k == 0 and b > 1:
+            forward(0)
+            forward_core(0)
+        for u in units[k]:
+            if u > 0 or b > 1:
+                arrive(X.at[every, unit(u)], core_r.at[u])
 
     NT = min(512, U)
     NS = min(256, S)
@@ -439,25 +443,25 @@
                     else:
                         tc[m, rs, n * NS : (n + 1) * NS] = part.astype(BF16)
                 if not mine_side:
-                    send(tc.at[m, rs], fc.at[m, rs], rc_s.at[m, k], rc_r.at[m, k], core_peer)
+                    send(tc.at[m, rs], fc.at[m, rs], "tc", sum_r.at[index_of[k]], core_peer)
 
     def reduce_core(k):
         rs = span_rows(k)
+        arrive(fc.at[every, rs], sum_r.at[index_of[k]])
         for m in list(range(1, NY)) + [0]:
-            arrive(fc.at[m, rs], rc_r.at[m, k])
             total = own[m, rs] + fc[m, rs].astype(F32)
             if m == 0:
                 own[0, rs] = total
             else:
                 ys[m, rs] = total.astype(BF16)
-                send(ys.at[m, rs], yr.at[m, rs], ry_s.at[m, k], ry_r.at[m, k], y_peer(m))
+                send(ys.at[m, rs], yr.at[m, rs], "ys", ysum_r.at[index_of[k]], y_peer(m))
 
     def reduce_y(k):
         j0, n = blocks[k]
         rs = span_rows(k)
         total = own[0, rs]
+        arrive(yr.at[others, rs], ysum_r.at[index_of[k]])
         for m in range(1, NY):
-            arrive(yr.at[m, rs], ry_r.at[m, k])
             total = total + yr[m, rs].astype(F32)
         done = total.astype(BF16).reshape(n, C, S)
         for i in range(n):
@@ -466,11 +470,11 @@
                 ret[0] = done[0]
             else:
                 fin[j] = done[i]
-                send(fin.at[j], ret.at[j], rt_s.at[j], rt_r.at[k], ep_peer(j))
+                send(fin.at[j], ret.at[j], "fin", ret_r.at[index_of[k]], ep_peer(j))
 
     def combine(k, place):
         if not local_only(k):
-            arrive(ret.at[span(k)], rt_r.at[k])
+            arrive(ret.at[span(k)], ret_r.at[index_of[k]])
         j0, n = blocks[k]
         size = n * C
         block = ret[j0 : j0 + n].reshape(size, S)
@@ -528,8 +532,7 @@
 
         @pl.when(e > 0)
         def _():
-            for i in range(3):
-                arrive(rims[i][1], rim_r.at[i])
+            arrive(rim, once_r.at[1])
 
     def ssd(g):
         run, run_t, step, to_end = (mix[n] for n in ("run", "run_t", "step", "to_end"))
@@ -568,8 +571,8 @@
     def state_exchange():
         st16[0] = state[0:half].astype(BF16)
         st16[1] = state[half:STATE].astype(BF16)
-        send(st16.at[1 - side], peerst, st_s.at[0], st_r.at[0], ep_peer(1))
-        send(dec_v, peerdec, st_s.at[1], st_r.at[1], ep_peer(1))
+        send(st16.at[1 - side], peerst, "st16", state_r.at[0], ep_peer(1))
+        send(dec_v, peerdec, "dec", state_r.at[1], ep_peer(1))
 
     behind = (jnp.maximum(e - 2, 0), t)
     ahead = (jnp.minimum(e + 2, E - 1), t)
@@ -577,8 +580,8 @@
     def chain(low, high):
         @pl.when((group >= low) & (group < high))
         def _():
-            arrive(peerst, st_r.at[0])
-            arrive(peerdec, st_r.at[1])
+            arrive(peerst, state_r.at[0])
+            arrive(peerdec, state_r.at[1])
             own_half = st16[side].astype(F32)
             other = peerst[...].astype(F32)
             own_dec = dec_v[0:1]
@@ -591,7 +594,7 @@
 
             @pl.when(group > 0)
             def _():
-                arrive(chin, st_r.at[2])
+                arrive(chin, state_r.at[2])
 
             @pl.when(group == 0)
             def _():
@@ -603,14 +606,14 @@
             @pl.when(group < pairs_count - 1)
             def _():
                 chout[...] = (e1 * d1 + s1).astype(BF16)
-                rcopy(chout, chin, st_s.at[2], st_r.at[2], ahead).start()
+                send(chout, chin, "chain", state_r.at[2], ahead)
 
             enter[side] = jnp.where(left, e0, e1).astype(BF16)
             esend[...] = jnp.where(left, e1, e0).astype(BF16)
-            rcopy(esend, enter.at[side], st_s.at[3], st_r.at[3], ep_peer(1)).start()
+            send(esend, enter.at[side], "enter", state_r.at[3], ep_peer(1))
 
     def gate_norm():
-        arrive(enter.at[1 - side], st_r.at[3])
+        arrive(enter.at[1 - side], state_r.at[3])
         entered = enter[...].reshape(STATE, channels)
         for g in range(groups):
             cols = slice(g * wide, (g + 1) * wide)
@@ -634,22 +637,22 @@
                 aown[m, :, n * NA : (n + 1) * NA] = jnp.where(c == 0, low, high)
                 atc[m, :, n * NA : (n + 1) * NA] = jnp.where(c == 0, high, low).astype(BF16)
         for m in list(range(1, NY)) + [0]:
-            send(atc.at[m], afc.at[m], mc_s.at[m], mc_r.at[m], core_peer)
+            send(atc.at[m], afc.at[m], "atc", once_r.at[2], core_peer)
 
     def mix_core():
+        arrive(afc, once_r.at[2])
         for m in list(range(1, NY)) + [0]:
-            arrive(afc.at[m], mc_r.at[m])
             total = aown[m] + afc[m].astype(F32)
             if m == 0:
                 aown[0] = total
             else:
                 ays[m] = total.astype(BF16)
-                send(ays.at[m], ayr.at[m], my_s.at[m], my_r.at[m], y_peer(m))
+                send(ays.at[m], ayr.at[m], "ays", once_r.at[3], y_peer(m))
 
     def mix_y():
         total = aown[0]
+        arrive(ayr.at[others], once_r.at[3])
         for m in range(1, NY):
-            arrive(ayr.at[m], my_r.at[m])
             total = total + ayr[m].astype(F32)
         outa_ref[...] = total.astype(BF16)
 
@@ -701,19 +704,29 @@
             steps[name](*which)
 
     with jax.named_scope("drain"):
-        for copy in sends:
-            copy.wait_send()
-
-    @pl.when(e < E - 1)
-    def _():
-        for i in range(3):
-            rim_copy(i).wait_send()
-
-    @pl.when(group < pairs_count - 1)
-    def _():
-        rcopy(chout, chin, st_s.at[2], st_r.at[2], ahead).wait_send()
-
-    rcopy(esend, enter.at[side], st_s.at[3], st_r.at[3], ep_peer(1)).wait_send()
+        far = E - 1
+        drain("out", out.at[pl.ds(1, far)])
+        if TWICE > 0:
+            drain("out1", out1.at[others])
+            far -= b
+        drain("y", X.at[pl.ds(0, NY - 1), pl.ds(0, far)])
+        drain("core", X.at[every, pl.ds(1, E - 1)])
+        drain("tc", tc)
+        drain("ys", ys.at[others])
+        drain("fin", fin.at[pl.ds(1, E - 1)])
+        drain("st16", peerst)
+        drain("dec", dec_v)
+        drain("enter", esend)
+        drain("atc", atc)
+        drain("ays", ays.at[others])
+
+        @pl.when(e < E - 1)
+        def _():
+            drain("rim", rim)
+
+        @pl.when(group < pairs_count - 1)
+        def _():
+            drain("chain", chout)
 
 
 def local(
@@ -823,25 +836,13 @@
             vmem((NY, R, width_a), BF16),
             vmem((NY, R, width_a), BF16),
             dma((len(far),)),
-            dma((NY, E)),
+            dma((len(KINDS),)),
             dma((UNITS,)),
-            dma((NY,)),
-            dma((NY, UNITS)),
-            dma((NY, UNITS)),
-            dma((NY, UNITS)),
-            dma((NY, UNITS)),
-            dma((NY, UNITS)),
-            dma((NY, UNITS)),
-            dma((NY, UNITS)),
-            dma((NY, UNITS)),
-            dma((E,)),
             dma((UNITS,)),
-            dma((NY,)),
-            dma((NY,)),
-            dma((NY,)),
-            dma((NY,)),
-            dma((3,)),
-            dma((3,)),
+            dma((UNITS,)),
+            dma((len(GROUPS),)),
+            dma((len(GROUPS),)),
+            dma((len(GROUPS),)),
             dma((4,)),
             dma((4,)),
         ],

time: 64.5 us -> 61.1 us (0.947)
  Pallas kernels: 62.3 us -> 58.8 us
    pallas_call x1, Pallas kernels: 62.3 us -> 58.8 us  [local(): pl.pallas_call(functools.partial(layer_kernel, E, T), in_specs=[pl.BlockS...]
where the time goes in v3:
time: 61.1 us; the launch traced here: 60.9 us
  Pallas kernels  58.8 us (96%)
  local copies, waits for them, and re-layouts  1.41 us (2%)
  between operations  0.65 us (1%)
    pallas_call x1, Pallas kernels, local(): pl.pallas_call(functools.partial(layer_kernel, E, T), in_specs=[pl.BlockS...  58.8 us
    unnamed x2, local copies, waits for them, and re-layouts  1.41 us

profile of v3, /device:TPU:0, one launch (start us, length us, event | category | flops | bytes accessed | tf_op | source)
XLA Modules:
  0.0 60.9 jit_solution(12487285851845934430)
XLA Ops:
  0.6 58.8 %layer.1 = (bf16[64,2048]{1,0:T(8,128)(2,1)S(1)}, bf16[256,512]{1,0:T(8,128)(2,1)S(1)}) custom-call(s32[2,256]{1,0:T(2,128)} %bitcast.12, f32[2,256]{1,0:T(2,128)} %bitcast.13, bf16[256,2048]{1,0:T(8,128)(2,1)} %act_h.1, bf16[2048]{0:T(1024)(128)(2,1)} %bgain_h.1, bf16[256,1024]{1,0:T(8,128)(2,1)} %x_h.1, bf16[256,512]{1,0:T(8,128)(2,1)} %b_h.1, ...), custom_call_target="tpu_custom_call" | custom-call | tf_op jit(solution)/shard_map/layer/pallas_call | solution.py:796
  59.5 0.7 %copy.25 = bf16[64,2048]{1,0:T(8,128)(2,1)} copy(bf16[64,2048]{1,0:T(8,128)(2,1)S(1)} %get-tuple-element.2) | data formatting | bytes 524288
  60.2 0.7 %copy.26 = bf16[256,512]{1,0:T(8,128)(2,1)} copy(bf16[256,512]{1,0:T(8,128)(2,1)S(1)} %get-tuple-element.3) | data formatting | bytes 524288

commit v4 on v3

--- a/solution.py
+++ b/solution.py
@@ -24,81 +24,82 @@
 GROUPS = ((0, 1), (1, 1), (2, 2), (4, 1), (5, 1), (6, 1), (7, 1))
 KINDS = ("out", "out1", "y", "core", "tc", "ys", "fin", "rim", "st16", "dec", "chain", "enter", "atc", "ays")
 TWICE = 1
-SENDING = (2, 4, 1, 5, 3, 7, 6)
+SENDING = (2, 4, 1, 5, 6, 3, 7)
 
 ORDER = (
+    ("mp",),
     ("rd", 0),
     ("lw",),
     ("gu", 0),
-    ("mp",),
+    ("ld",),
+    ("dn", 0),
+    ("ssd", 0),
+    ("fw", 1),
+    ("fc", 1),
+    ("rc", 0),
+    ("fw", 4),
     ("fw", 2),
-    ("ssd", 0),
-    ("fw", 4),
     ("ssd", 1),
-    ("fc", 1),
-    ("fw", 1),
     ("ssd", 2),
     ("ssd", 3),
+    ("rd", 1),
     ("sx",),
+    ("gu", 1),
+    ("fw", 5),
     ("fc", 4),
-    ("rd", 1),
+    ("dn", 1),
+    ("fc", 2),
     ("fw", 3),
-    ("dn", 0),
-    ("fw", 5),
-    ("gu", 1),
+    ("ch", 0),
     ("rd", 4),
-    ("ch", 0),
-    ("rc", 0),
-    ("dn", 1),
     ("gu", 4),
-    ("rc", 1),
+    ("fw", 7),
     ("fc", 5),
     ("dn", 4),
-    ("fc", 2),
+    ("fc", 3),
+    ("rd", 5),
+    ("ch", 1),
     ("fw", 6),
-    ("ch", 1),
-    ("rd", 5),
-    ("fc", 3),
     ("gu", 5),
     ("rc", 4),
     ("dn", 5),
-    ("fw", 7),
     ("rd", 2),
     ("gu", 2),
     ("fc", 6),
+    ("ch", 2),
     ("rc", 5),
-    ("ch", 2),
-    ("ry", 1),
     ("dn", 2),
+    ("fc", 7),
+    ("ry", 4),
     ("rd", 6),
-    ("ry", 4),
     ("gu", 6),
+    ("rc", 2),
     ("dn", 6),
-    ("fc", 7),
+    ("rd", 7),
     ("ch", 3),
-    ("rc", 6),
     ("ry", 0),
     ("ry", 5),
-    ("rc", 2),
-    ("rd", 7),
     ("gu", 7),
     ("dn", 7),
+    ("rc", 6),
+    ("cb", 0),
+    ("rc", 7),
     ("lr",),
     ("gn",),
-    ("rc", 7),
+    ("ry", 2),
+    ("pj",),
+    ("rc", 1),
     ("ry", 6),
+    ("ry", 7),
+    ("mc",),
+    ("ry", 1),
+    ("cb", 2),
+    ("cb", 4),
     ("cb", 1),
-    ("pj",),
-    ("ry", 2),
+    ("cb", 7),
     ("cb", 5),
-    ("mc",),
-    ("ry", 7),
+    ("my",),
     ("cb", 6),
-    ("cb", 0),
-    ("cb", 4),
-    ("cb", 2),
-    ("my",),
-    ("cb", 7),
 )
 
 
@@ -147,9 +148,9 @@
     wu_h,
     wd_h,
     wr_h,
-    offset_s,
-    speed_s,
-    bypass_s,
+    offset_h,
+    speed_h,
+    bypass_h,
     outa_ref,
     outb_ref,
     picks_v,
@@ -170,6 +171,9 @@
     wu_v,
     wd_v,
     wr_v,
+    offset_s,
+    speed_s,
+    bypass_s,
     nb,
     out,
     out1,
@@ -255,6 +259,9 @@
         (valve_h, valve_v),
         (again_h, again_v),
         (wr_h, wr_v),
+        (offset_h, offset_s),
+        (speed_h, speed_s),
+        (bypass_h, bypass_s),
     ]
     loads = {}
     for i, (src, dst) in enumerate(pairs):
@@ -515,6 +522,8 @@
     lane128 = lax.broadcasted_iota(jnp.int32, (rows, LANES), 1)
 
     def mix_prepare():
+        for i in (18, 19, 20):
+            loads[i].wait()
         z = pre_v[...] + column(offset_s)
         step_t = jnp.maximum(z, 0.0) + jnp.log1p(jnp.exp(-jnp.abs(z)))
         decay_t = -jnp.exp(column(speed_s)) * step_t + extra_v[...]
@@ -529,10 +538,6 @@
         mix["run_t"] = dot_last(decay_t, tri, HIGHEST)
         mix["step"] = dot_last(eye, step_t, HIGHEST)
         mix["to_end"] = jnp.exp(last - run)
-
-        @pl.when(e > 0)
-        def _():
-            arrive(rim, once_r.at[1])
 
     def ssd(g):
         run, run_t, step, to_end = (mix[n] for n in ("run", "run_t", "step", "to_end"))
@@ -660,14 +665,24 @@
     seen = []
 
     def load_weights():
-        for i in (12, 13, 14):
+        for i in (12, 13):
             loads[i].wait()
+
+    def load_down():
+        loads[14].wait()
 
     def load_rest():
         for i in (15, 16, 17):
             loads[i].wait()
 
+    def await_rim():
+        @pl.when(e > 0)
+        def _():
+            arrive(rim, once_r.at[1])
+
     def ssd_part(i):
+        if i == 0:
+            await_rim()
         for g in range(i * groups // 4, (i + 1) * groups // 4):
             ssd(g)
 
@@ -693,6 +708,7 @@
         "sx": state_exchange,
         "ch": chain_part,
         "lw": load_weights,
+        "ld": load_down,
         "lr": load_rest,
         "gn": gate_norm,
         "pj": project,
@@ -727,6 +743,17 @@
         @pl.when(group < pairs_count - 1)
         def _():
             drain("chain", chout)
+
+
+def hand_over(a_ref, b_ref, outa_ref, outb_ref, sem):
+    copies = [
+        pltpu.make_async_copy(a_ref, outa_ref, sem.at[0]),
+        pltpu.make_async_copy(b_ref, outb_ref, sem.at[1]),
+    ]
+    for copy in copies:
+        copy.start()
+    for copy in copies:
+        copy.wait()
 
 
 def local(
@@ -791,12 +818,12 @@
     ]
     near = [stride_offset_vector, attenuation_speed_exponent, bypass_coef_vector]
     landing = [pltpu.VMEM(a.shape, a.dtype) for a in far]
+    landing += [pltpu.SMEM(a.shape, a.dtype) for a in near]
     dma = pltpu.SemaphoreType.DMA
     vmem = pltpu.VMEM
-    return pl.pallas_call(
+    mixed = pl.pallas_call(
         functools.partial(layer_kernel, E, T),
-        in_specs=[pl.BlockSpec(memory_space=pl.ANY)] * len(far)
-        + [pl.BlockSpec(memory_space=pltpu.SMEM)] * len(near),
+        in_specs=[pl.BlockSpec(memory_space=pl.ANY)] * len(far + near),
         out_specs=[pl.BlockSpec(memory_space=pltpu.VMEM)] * 2,
         out_shape=[pltpu.VMEM((R, width_a), BF16), pltpu.VMEM((tok, S), BF16)],
         scratch_shapes=landing
@@ -835,7 +862,7 @@
             vmem((NY, R, width_a), F32),
             vmem((NY, R, width_a), BF16),
             vmem((NY, R, width_a), BF16),
-            dma((len(far),)),
+            dma((len(far + near),)),
             dma((len(KINDS),)),
             dma((UNITS,)),
             dma((UNITS,)),
@@ -851,6 +878,15 @@
         ),
         name="layer",
     )(*far, *near)
+    mixed = [pltpu.with_memory_space_constraint(a, pltpu.VMEM) for a in mixed]
+    return pl.pallas_call(
+        hand_over,
+        in_specs=[pl.BlockSpec(memory_space=pltpu.VMEM)] * 2,
+        out_specs=[pl.BlockSpec(memory_space=pl.ANY)] * 2,
+        out_shape=[jax.ShapeDtypeStruct(a.shape, a.dtype) for a in mixed],
+        scratch_shapes=[dma((2,))],
+        name="hand_over",
+    )(*mixed)
 
 
 def solution(mesh):

time: 61.1 us -> 59.4 us (0.972)
  local copies, waits for them, and re-layouts: 1.41 us -> 0 us
    unnamed x2 -> x0, local copies, waits for them, and re-layouts: 1.41 us -> none
    pallas_call x1, Pallas kernels: 58.8 us -> 57.6 us  [local(): pl.pallas_call(functools.partial(layer_kernel, E, T), in_specs=[pl.BlockS...]
    pallas_call x0 -> x1, Pallas kernels: none -> 0.81 us  [local(): pl.pallas_call(hand_over, in_specs=[pl.BlockSpec(memory_space=pltpu.VMEM)...]
where the time goes in v4:
time: 59.4 us; the launch traced here: 59.2 us
  Pallas kernels  58.4 us (98%)
  between operations  0.81 us (1%)
    pallas_call x1, Pallas kernels, local(): pl.pallas_call(functools.partial(layer_kernel, E, T), in_specs=[pl.BlockS...  57.6 us

profile of v4, /device:TPU:0, one launch (start us, length us, event | category | flops | bytes accessed | tf_op | source)
XLA Modules:
  0.0 59.2 jit_solution(9563981174094408244)
XLA Ops:
  0.6 57.6 %layer.1 = (bf16[64,2048]{1,0:T(8,128)(2,1)S(1)}, bf16[256,512]{1,0:T(8,128)(2,1)S(1)}) custom-call(s32[2,256]{1,0:T(2,128)} %bitcast.12, f32[2,256]{1,0:T(2,128)} %bitcast.13, bf16[256,2048]{1,0:T(8,128)(2,1)} %act_h.1, bf16[2048]{0:T(1024)(128)(2,1)} %bgain_h.1, bf16[256,1024]{1,0:T(8,128)(2,1)} %x_h.1, bf16[256,512]{1,0:T(8,128)(2,1)} %b_h.1, ...), custom_call_target="tpu_custom_call" | custom-call | tf_op jit(solution)/shard_map/layer/pallas_call | solution.py:824
  58.2 0.8 %hand_over.1 = (bf16[64,2048]{1,0:T(8,128)(2,1)}, bf16[256,512]{1,0:T(8,128)(2,1)}) custom-call(bf16[64,2048]{1,0:T(8,128)(2,1)S(1)} %get-tuple-element.4.a_ref, bf16[256,512]{1,0:T(8,128)(2,1)S(1)} %get-tuple-element.5.b_ref), custom_call_target="tpu_custom_call" | custom-call | tf_op jit(solution)/shard_map/hand_over/pallas_call | solution.py:882
